TPU v7x, 512 devices: a whole 4x4x16 slice. The times are simulated.
512 devices in a mesh: sp: 64 (over z, y), tp: 8 (over x, core).
Axes of the slice: x: 4, y: 4, z: 16, core: 2. Of those that a mesh axis runs over, the one named last changes fastest.
Arguments:
- residual: bfloat16 [8192, 2048], P('sp'), may hold values from -6 to 6
- query_nope: bfloat16 [8192, 8, 128], P('sp', 'tp'), may hold values from -6 to 6
- query_rope: bfloat16 [8192, 8, 64], P('sp', 'tp'), may hold values from -64 to 64
- latent: bfloat16 [8192, 256], P('sp'), may hold values from -6 to 6
- rope_key: bfloat16 [8192, 64], P('sp'), may hold values from -64 to 64
- kv_gain: bfloat16 [256], replicated, may hold values from 0.099609375 to 1.8984375
- key_up: bfloat16 [256, 8, 128], replicated, may hold values from -0.375 to 0.375
- value_up: bfloat16 [256, 8, 128], replicated, may hold values from -0.375 to 0.375
- out_weight: bfloat16 [1024, 2048], P('tp'), may hold values from -0.1875 to 0.1875
- post_gain: bfloat16 [2048], replicated, may hold values from 0.099609375 to 1.8984375
- pre_gain: bfloat16 [2048], replicated, may hold values from 0.099609375 to 1.8984375
- ffn_gain: bfloat16 [2048], replicated, may hold values from 0.099609375 to 1.8984375
- up_value: bfloat16 [2048, 5632], P('sp', 'tp'), may hold values from -0.125 to 0.125
- up_gate: bfloat16 [2048, 5632], P('sp', 'tp'), may hold values from -0.125 to 0.125
- conv_value: bfloat16 [3, 5632], replicated, may hold values from -3.5 to 3.5
- conv_gate: bfloat16 [3, 5632], replicated, may hold values from -3.5 to 3.5
- down_weight: bfloat16 [5632, 2048], P('tp', 'sp'), may hold values from -0.078125 to 0.078125
Outputs:
- layer_out: bfloat16 [8192, 2048], P(('sp', 'tp'))
All inputs are finite; a program needn't handle non-finite values.
Results may differ from a plain program's by a relative error of at most 0.02.
Values may be sent and summed in bfloat16 or wider, within the bound.
A program may use at most 128 MiB of HBM per device.

v0:
```python
import jax
import jax.numpy as jnp
from jax import lax
from jax.sharding import Mesh
from jax.sharding import PartitionSpec as P

GRID = 64
SP = ("sp_0", "sp_1")
SP_TP = ("sp_0", "sp_1", "tp")


epsilon = 1e-06
rope_base = 10000.0


def side_by_side(arrays, axis, dim, along):
    both = jnp.concatenate(arrays, axis=along)
    whole, at, outs = (lax.all_gather(both, axis, axis=dim, tiled=True), 0, [])
    for a in arrays:
        outs.append(lax.slice_in_dim(whole, at, at + a.shape[along], axis=along))
        at += a.shape[along]
    return tuple(outs)


def sent_to_all(x, axis):
    size = lax.axis_size(axis)
    return lax.all_to_all(jnp.broadcast_to(x[None], (size, *x.shape)), axis, 0, 0, tiled=True)


def taken_together(x, axis):
    return sent_to_all(x, axis).astype(jnp.float32).sum(axis=0)


def joined_along(pieces, dim):
    pieces = jnp.moveaxis(pieces, 0, dim)
    shape = pieces.shape
    return pieces.reshape(*shape[:dim], shape[dim] * shape[dim + 1], *shape[dim + 2 :])


def stacked_from(x, axes, order):
    pieces = x[None]
    for k in order:
        pieces = lax.all_gather(pieces, axes[k], axis=0, tiled=True)
    current = [lax.axis_size(axes[k]) for k in reversed(order)]
    pieces = pieces.reshape(*current, *x.shape)
    turned = sorted(range(len(order)), key=lambda place: order[len(order) - 1 - place])
    return pieces.transpose(*turned, *range(len(order), pieces.ndim)).reshape(-1, *x.shape)


def gathered_by_axis(x, axes, order, dim):
    return joined_along(stacked_from(x, axes, order), dim)


def extended(x, sides, width):
    for axis, dim in sides:
        size, length = (lax.axis_size(axis), x.shape[dim])
        up = [(i, (i + 1) % size) for i in range(size - 1)]
        down = [(j, i) for i, j in up]
        last = lax.slice_in_dim(x, length - width, length, axis=dim)
        initial = lax.slice_in_dim(x, 0, width, axis=dim)
        before = lax.ppermute(last, axis, up)
        after = lax.ppermute(initial, axis, down)
        x = jnp.concatenate([before, x, after], axis=dim)
    return x


def whole_of(x, axes, dim):
    for axis in reversed(axes):
        x = lax.all_gather(x, axis, axis=dim, tiled=True)
    return x


def split_up(x, dim, size):
    shape = x.shape
    pieces = x.reshape(*shape[:dim], size, shape[dim] // size, *shape[dim + 1 :])
    return jnp.moveaxis(pieces, dim, 0)


def sum_at_owner(x, axis, dim):
    size = lax.axis_size(axis)
    pieces = lax.all_to_all(split_up(x, dim, size), axis, 0, 0, tiled=True)
    return jnp.sum(pieces.astype(jnp.float32), axis=0)


def rms_norm(values, gain):
    return (
        values
        * lax.rsqrt(jnp.mean(values * values, axis=-1, keepdims=True) + epsilon)
        * gain.astype(jnp.float32)
    )


def widened(values):
    return lax.optimization_barrier(values.astype(jnp.bfloat16)).astype(jnp.float32)


def rotate(values, positions):
    pair_count = values.shape[-1] // 4
    frequency = rope_base ** (-jnp.arange(pair_count, dtype=jnp.float32) / pair_count)
    grid_rows = (positions // GRID).astype(jnp.float32)
    grid_cols = (positions % GRID).astype(jnp.float32)
    angles = jnp.stack([grid_rows, grid_cols], axis=-1)[:, :, None] * frequency
    table_shape = (angles.shape[0],) + (1,) * (values.ndim - 2) + angles.shape[1:]
    cosine = jnp.cos(angles).reshape(table_shape)
    sine = jnp.sin(angles).reshape(table_shape)
    halves = values.reshape(values.shape[:-1] + (2, 2, pair_count))
    leading = halves[..., 0, :]
    trailing = halves[..., 1, :]
    turned = jnp.stack(
        [leading * cosine - trailing * sine, trailing * cosine + leading * sine], axis=-2
    )
    return turned.reshape(values.shape)


def body(
    residual,
    query_nope,
    query_rope,
    latent,
    rope_key,
    kv_gain,
    key_up,
    value_up,
    out_weight,
    post_gain,
    pre_gain,
    ffn_gain,
    up_value,
    up_gate,
    conv_value,
    conv_gate,
    down_weight,
):
    tok_rows = residual.shape[0]
    heads_dev = query_nope.shape[1]
    value_width = value_up.shape[2]
    tp_index = lax.axis_index("tp")
    positions = lax.axis_index(SP) * tok_rows + jnp.arange(tok_rows, dtype=jnp.int32)
    score_scale = (query_nope.shape[2] + query_rope.shape[2]) ** (-0.5)
    normed = rms_norm(latent.astype(jnp.float32), kv_gain).astype(jnp.bfloat16)
    key_turn = rotate(rope_key.astype(jnp.float32), positions).astype(jnp.bfloat16)
    query_turn = rotate(query_rope.astype(jnp.float32), positions).astype(jnp.bfloat16)
    key_local = lax.dynamic_slice_in_dim(key_up, tp_index * heads_dev, heads_dev, 1)
    value_local = lax.dynamic_slice_in_dim(value_up, tp_index * heads_dev, heads_dev, 1)
    pieces = side_by_side((normed, key_turn), SP, 0, 1)
    keys_nope = jnp.einsum(
        "nc,chd->nhd", pieces[0], key_local, preferred_element_type=jnp.float32
    ).astype(jnp.bfloat16)
    values_part = jnp.einsum(
        "nc,chd->nhd", pieces[0], value_local, preferred_element_type=jnp.float32
    ).astype(jnp.bfloat16)
    row_max = jnp.full((heads_dev, tok_rows), -1e30, jnp.float32)
    scores = (
        jnp.einsum("qhd,khd->hqk", query_nope, keys_nope, preferred_element_type=jnp.float32)
        + jnp.einsum("qhd,kd->hqk", query_turn, pieces[1], preferred_element_type=jnp.float32)
    ) * score_scale
    new_max = jnp.maximum(row_max, jnp.max(scores, axis=-1))
    weights = jnp.exp(scores - new_max[:, :, None])
    totals = jnp.sum(weights, axis=-1)
    weighted = jnp.einsum(
        "hqk,khd->hqd",
        weights.astype(jnp.bfloat16),
        values_part,
        preferred_element_type=jnp.float32,
    )
    attended = (weighted / totals[:, :, None]).astype(jnp.bfloat16)
    attended = jnp.transpose(attended, (1, 0, 2)).reshape(tok_rows, heads_dev * value_width)
    row_share = tok_rows // lax.axis_size("tp")
    summed = taken_together(
        jnp.dot(attended, out_weight, preferred_element_type=jnp.float32).astype(jnp.bfloat16), "tp"
    ).astype(jnp.float32)
    stream_all = widened(residual.astype(jnp.float32) + rms_norm(widened(summed), post_gain))
    inputs = rms_norm(stream_all, pre_gain).astype(jnp.bfloat16)
    stream_wide = lax.dynamic_slice_in_dim(stream_all, tp_index * row_share, row_share, 0)
    ff_dev = up_value.shape[1]
    up_joined = jnp.concatenate([up_value, up_gate], axis=1)
    up_whole = gathered_by_axis(up_joined, SP, (0, 1), 0)
    up_pair = jnp.dot(inputs, up_whole, preferred_element_type=jnp.float32).astype(jnp.bfloat16)
    padded = extended(up_pair, ((SP, 0),), 1).astype(jnp.float32)
    channel_start = tp_index * ff_dev
    conv_taps = jnp.concatenate(
        [
            lax.dynamic_slice_in_dim(conv_value, channel_start, ff_dev, 1),
            lax.dynamic_slice_in_dim(conv_gate, channel_start, ff_dev, 1),
        ],
        axis=1,
    ).astype(jnp.float32)
    mixed_conv = (
        padded[:-2] * conv_taps[0] + padded[1:-1] * conv_taps[1] + padded[2:] * conv_taps[2]
    )
    hidden = (jax.nn.silu(mixed_conv[:, ff_dev:]) * mixed_conv[:, :ff_dev]).astype(jnp.bfloat16)
    down_whole = whole_of(down_weight, SP, 1)
    down_terms = jnp.dot(hidden, down_whole, preferred_element_type=jnp.float32)
    reduced = sum_at_owner(down_terms.astype(jnp.bfloat16), "tp", 0)
    return (stream_wide + rms_norm(widened(reduced), ffn_gain)).astype(jnp.bfloat16)


def solution(mesh):
    torus = Mesh(mesh.devices.reshape(16, 4, mesh.shape["tp"]), ("sp_0", "sp_1", "tp"))
    return jax.shard_map(
        body,
        mesh=torus,
        in_specs=(
            P(SP, None),
            P(SP, "tp", None),
            P(SP, "tp", None),
            P(SP, None),
            P(SP, None),
            P(),
            P(),
            P(),
            P("tp", None),
            P(),
            P(),
            P(),
            P(SP, "tp"),
            P(SP, "tp"),
            P(),
            P(),
            P("tp", SP),
        ),
        out_specs=P(SP_TP, None),
        check_vma=False,
    )
```

profile of v0, /device:TPU:1, one launch (start us, length us, event | category | flops | bytes accessed | tf_op | source)
XLA Modules:
  0.0 408.5 jit_solution(6371514957831806207)
XLA Ops:
  6.5 0.0 copy-start
  6.5 0.0 all-gather.12.cloned.1.call-start
  6.5 1.6 pad_maximum_fusion.1
  8.1 0.0 all-gather.12.cloned.1.call-update
  8.2 0.0 all-gather.6.cloned.1.call-start
  8.2 0.7 convert.20
  9.0 0.1 fusion.58
  9.2 0.1 copy.30
  9.3 0.7 convert_element_type.113
  9.9 0.9 fusion.37
  10.9 0.9 fusion.39
  11.8 0.7 pad_maximum_fusion
  12.5 0.0 all-gather.6.cloned.1.call-update
  12.5 0.0 all-gather.8.cloned.1.call-start
  12.6 64.1 %all-gather.12.cloned.1.call-done = bf16[512,1408]{1,0:T(8,128)(2,1)} async-done(((bf16[32,1408]{1,0:T(8,128)(2,1)}), bf16[512,1408]{1,0:T(8,128)(2,1)}) %all-gather.12.cloned.1.call-update) | async-done | bytes 1441808 | tf_op jit(solution)/shard_map/all_gather | solution.py:43
  76.7 0.0 all-gather.8.cloned.1.call-update
  76.7 0.7 convert.21
  77.4 0.1 fusion.54
  77.6 0.0 copy-start.3
  77.6 1.5 constant_dynamic-slice_fusion.2
  79.1 149.7 %all-gather.6.cloned.1.call-done = bf16[8192,320]{1,0:T(8,128)(2,1)} async-done(((bf16[128,320]{1,0:T(8,128)(2,1)}), bf16[8192,320]{1,0:T(8,128)(2,1)}) %all-gather.6.cloned.1.call-update) | async-done | bytes 5242896 | tf_op jit(solution)/shard_map/all_gather | solution.py:18
  228.8 4.2 %convolution_bitcast_fusion = f32[1,128,8192]{1,2,0:T(8,128)} fusion(bf16[128,64]{0,1:T(8,128)(2,1)S(1)} %bitcast.54, bf16[8192,320]{1,0:T(8,128)(2,1)} %all-gather.6.cloned.1.call-done), kind=kOutput, calls=%fused_computation | convolution fusion | flops 134217728 | bytes 6307840 | tf_op jit(solution)/shard_map/qhd,kd->hqk/dot_general | solution.py:155
  233.0 0.0 copy-done.3
  233.0 7.6 %fusion.67 = (f32[128]{0:T(128)S(1)}, f32[1,128,8192]{1,2,0:T(8,128)}) fusion(f32[1,128,8192]{1,2,0:T(8,128)} %convolution_bitcast_fusion, bf16[128,1,128]{2,0,1:T(8,128)(2,1)S(1)} %copy-done.3, bf16[8192,320]{1,0:T(8,128)(2,1)} %all-gather.6.cloned.1.call-done, bf16[256,1,128]{2,1,0:T(2,128)(2,1)S(1)} %get-tuple-element.19), kind=kOutput, calls=%fused_computation.104 | convolution fusion | flops 809500544 | bytes 12681728 | tf_op jit(solution)/shard_map/qhd,khd->hqk/dot_general | solution.py:154
  240.6 3.3 fusion.2
  243.8 5.7 %fusion.20 = bf16[128,128]{1,0:T(8,128)(2,1)S(1)} fusion(bf16[8192,320]{1,0:T(8,128)(2,1)} %all-gather.6.cloned.1.call-done, f32[1,128,8192]{1,2,0:T(8,128)} %get-tuple-element.15, f32[128]{0:T(128)S(1)} %broadcast_maximum_fusion, bf16[256,1,128]{2,1,0:T(2,128)(2,1)S(1)} %get-tuple-element.18, f32[128]{0:T(128)S(1)} %fusion.2), kind=kOutput, calls=%fused_computation.21 | convolution fusion | flops 808484864 | bytes 8487936 | tf_op jit(solution)/shard_map/hqk,khd->hqd/dot_general | solution.py:160
  249.6 0.0 copy-done
  249.6 0.3 convolution_convert_fusion.3
  249.9 2.5 broadcast_in_dim.7
  252.4 0.0 copy-start.2
  252.4 14.1 %all-to-all-start = ((bf16[8,128,2048]{2,1,0:T(8,128)(2,1)}), bf16[8,128,2048]{2,1,0:T(8,128)(2,1)}, u32[]{:S(2)}, u32[]{:S(2)}) async-start(bf16[8,128,2048]{2,1,0:T(8,128)(2,1)} %broadcast_in_dim.7), calls=%async_computation | async-start | bytes 8388608 | tf_op jit(solution)/shard_map/all_to_all | solution.py:27
  266.4 0.0 all-gather.10.cloned.1.call-start
  266.4 0.0 copy-done.2
  266.5 12.0 %all_gather.18 = bf16[704,128]{0,1:T(8,128)(2,1)} all-gather(bf16[704,32]{0,1:T(8,128)(2,1)S(1)} %copy-done.2), channel_id=1, replica_groups=mesh['sp_0'=16,'sp_1'=4,'tp'=8] {'sp_1'}, dimensions={1}, use_global_device_ids=true | all-gather | bytes 225280 | tf_op jit(solution)/shard_map/all_gather | solution.py:69
  278.5 0.0 all-gather.10.cloned.1.call-update
  278.5 0.0 copy-done.4
  278.5 0.0 copy-done.5
  278.5 0.8 constant_dynamic-slice_fusion
  279.3 25.3 %all-gather.8.cloned.1.call-done = bf16[64,32,1408]{2,1,0:T(8,128)(2,1)} async-done(((bf16[16,32,1408]{2,1,0:T(8,128)(2,1)}), bf16[64,32,1408]{2,1,0:T(8,128)(2,1)}) %all-gather.8.cloned.1.call-update) | async-done | bytes 5767184 | tf_op jit(solution)/shard_map/all_gather | solution.py:43
  304.7 5.8 %copy.33 = bf16[16,4,32,1408]{3,2,1,0:T(8,128)(2,1)} copy(bf16[16,4,32,1408]{3,2,0,1:T(8,128)(2,1)} %bitcast.52) | data formatting | bytes 11534336 | tf_op jit(solution)/shard_map/transpose | solution.py:47
  310.5 4.7 %all-to-all-done = bf16[8,128,2048]{2,1,0:T(8,128)(2,1)} async-done(((bf16[8,128,2048]{2,1,0:T(8,128)(2,1)}), bf16[8,128,2048]{2,1,0:T(8,128)(2,1)}, u32[]{:S(2)}, u32[]{:S(2)}) %all-to-all-start) | async-done | bytes 4194336 | tf_op jit(solution)/shard_map/all_to_all | solution.py:27
  315.3 3.0 reduce_sum.71
  318.2 0.2 fusion.25
  318.4 0.0 copy-done.1
  318.4 0.3 fusion.28
  318.7 0.2 multiply_reduce_fusion
  318.9 3.7 convolution_convert_fusion.4
  322.6 2.5 collective-permute-start
  325.1 1.3 collective-permute-start.1
  326.4 0.1 convert_reduce_fusion.1
  326.5 0.0 collective-permute-done
  326.5 3.3 collective-permute-done.1
  329.9 0.1 maximum_convert_fusion
  330.0 0.0 copy-start.6
  330.0 0.2 fusion.29
  330.2 43.6 %all-gather.10.cloned.1.call-done = bf16[704,2048]{0,1:T(8,128)(2,1)} async-done(((bf16[704,128]{0,1:T(8,128)(2,1)}), bf16[704,2048]{0,1:T(8,128)(2,1)}) %all-gather.10.cloned.1.call-update) | async-done | bytes 2883600 | tf_op jit(solution)/shard_map/all_gather | solution.py:69
  373.8 3.9 convolution_convert_fusion.2
  377.6 14.0 %all-to-all-start.1 = ((bf16[8,16,2048]{2,1,0:T(8,128)(2,1)}), bf16[8,16,2048]{2,1,0:T(8,128)(2,1)S(1)}, u32[]{:S(2)}, u32[]{:S(2)}) async-start(bf16[8,16,2048]{2,1,0:T(8,128)(2,1)} %bitcast.18), calls=%async_computation.1 | async-start | bytes 1048576 | tf_op jit(solution)/shard_map/all_to_all | solution.py:81
  391.6 0.0 copy-done.6
  391.6 0.1 convert_element_type.127
  391.8 9.2 %all-to-all-done.1 = bf16[8,16,2048]{2,1,0:T(8,128)(2,1)S(1)} async-done(((bf16[8,16,2048]{2,1,0:T(8,128)(2,1)}), bf16[8,16,2048]{2,1,0:T(8,128)(2,1)S(1)}, u32[]{:S(2)}, u32[]{:S(2)}) %all-to-all-start.1) | async-done | bytes 524320 | tf_op jit(solution)/shard_map/all_to_all | solution.py:81
  401.0 0.1 reduce_sum.74
  401.1 0.1 fusion.40
  401.2 0.7 fusion.43
  (17 shorter events, 0.1 us)
Async XLA Ops:
  6.5 243.0 %copy-start = (bf16[128,2048]{1,0:T(8,128)(2,1)S(1)}, bf16[128,2048]{1,0:T(8,128)(2,1)}, u32[]{:S(2)}) copy-start(bf16[128,2048]{1,0:T(8,128)(2,1)} %param.25) | copy-start | bytes 1572868
  6.5 70.1 %all-gather.12.cloned.1.call-start = ((), (), s32[]{:S(2)}) async-start(), calls=%async_computation.5 | async-start | bytes 1531904 | tf_op jit(solution)/shard_map/all_gather | solution.py:43
  8.2 220.6 %all-gather.6.cloned.1.call-start = ((), (), s32[]{:S(2)}) async-start(), calls=%async_computation.2 | async-start | bytes 6389760 | tf_op jit(solution)/shard_map/all_gather | solution.py:18
  12.5 292.2 %all-gather.8.cloned.1.call-start = ((), (), s32[]{:S(2)}) async-start(), calls=%async_computation.3 | async-start | bytes 7208960 | tf_op jit(solution)/shard_map/all_gather | solution.py:43
  77.6 155.4 %copy-start.3 = (bf16[128,1,128]{2,0,1:T(8,128)(2,1)S(1)}, bf16[128,1,128]{2,0,1:T(8,128)(2,1)}, u32[]{:S(2)}) copy-start(bf16[128,1,128]{2,0,1:T(8,128)(2,1)} %param.18) | copy-start | bytes 98308
  252.4 14.1 %copy-start.2 = (bf16[704,32]{0,1:T(8,128)(2,1)S(1)}, bf16[704,32]{0,1:T(8,128)(2,1)}, u32[]{:S(2)}) copy-start(bf16[704,32]{0,1:T(8,128)(2,1)} %param.33) | copy-start | bytes 135172
  252.4 26.1 %copy-start.4 = (bf16[2048]{0:T(1024)(128)(2,1)S(1)}, bf16[2048]{0:T(1024)(128)(2,1)}, u32[]{:S(2)}) copy-start(bf16[2048]{0:T(1024)(128)(2,1)} %param.26) | copy-start | bytes 12292
  252.4 26.1 %copy-start.5 = (bf16[2048]{0:T(1024)(128)(2,1)S(1)}, bf16[2048]{0:T(1024)(128)(2,1)}, u32[]{:S(2)}) copy-start(bf16[2048]{0:T(1024)(128)(2,1)} %param.27) | copy-start | bytes 12292
  252.4 62.9 %all-to-all-start = ((bf16[8,128,2048]{2,1,0:T(8,128)(2,1)}), bf16[8,128,2048]{2,1,0:T(8,128)(2,1)}, u32[]{:S(2)}, u32[]{:S(2)}) async-start(bf16[8,128,2048]{2,1,0:T(8,128)(2,1)} %broadcast_in_dim.7), calls=%async_computation | async-start | bytes 8388608 | tf_op jit(solution)/shard_map/all_to_all | solution.py:27
  266.4 107.3 %all-gather.10.cloned.1.call-start = ((), (), s32[]{:S(2)}) async-start(), calls=%async_computation.4 | async-start | bytes 3342336 | tf_op jit(solution)/shard_map/all_gather | solution.py:69
  310.5 7.9 %copy-start.1 = (bf16[128,2048]{1,0:T(8,128)(2,1)S(1)}, bf16[128,2048]{1,0:T(8,128)(2,1)}, u32[]{:S(2)}) copy-start(bf16[128,2048]{1,0:T(8,128)(2,1)} %param.17) | copy-start | bytes 1572868
  322.6 3.9 collective-permute-start
  325.1 4.8 %collective-permute-start.1 = (bf16[1,1408]{1,0:T(2,128)(2,1)S(1)}, bf16[1,1408]{1,0:T(2,128)(2,1)S(1)}, u32[]{:S(2)}, u32[]{:S(2)}) collective-permute-start(bf16[1,1408]{1,0:T(2,128)(2,1)S(1)} %get-tuple-element.9), channel_id=1, source_target_pairs={{8,0},{16,8},{24,16},{32,24},{40,32},{48,40},{56,48},{64,56},{72,6... | collective-permute-start | bytes 8456 | tf_op jit(solution)/shard_map/ppermute | solution.py:62
  330.0 61.7 %copy-start.6 = (bf16[2048]{0:T(1024)(128)(2,1)S(1)}, bf16[2048]{0:T(1024)(128)(2,1)}, u32[]{:S(2)}) copy-start(bf16[2048]{0:T(1024)(128)(2,1)} %param.28) | copy-start | bytes 12292
  377.6 23.4 %all-to-all-start.1 = ((bf16[8,16,2048]{2,1,0:T(8,128)(2,1)}), bf16[8,16,2048]{2,1,0:T(8,128)(2,1)S(1)}, u32[]{:S(2)}, u32[]{:S(2)}) async-start(bf16[8,16,2048]{2,1,0:T(8,128)(2,1)} %bitcast.18), calls=%async_computation.1 | async-start | bytes 1048576 | tf_op jit(solution)/shard_map/all_to_all | solution.py:81
Sparse Core Ops, SparseCore 0:
  9.4 67.2 all-gather.11
  79.6 149.0 all-gather.5
  230.9 73.7 all-gather.7
  306.6 67.1 all-gather.9
where the time goes:
time: 409 us; the launch traced here: 408 us
  waiting for transfers between devices  300 us (73%)
  starting transfers between devices  32 us (8%)
  matrix products  25.3 us (6%)
  other arithmetic  15 us (4%)
  between operations  13.4 us (3%)
  blocking collectives  12 us (3%)
  local copies, waits for them, and re-layouts  10.8 us (3%)
    all_gather x1, waiting for transfers between devices, side_by_side(): whole, at, outs = (lax.all_gather(both, axis, axis=dim, tiled=True), 0, [])  150 us
    all_gather x2, waiting for transfers between devices, stacked_from(): pieces = lax.all_gather(pieces, axes[k], axis=0, tiled=True)  89.5 us
    all_gather x1, waiting for transfers between devices, whole_of(): x = lax.all_gather(x, axis, axis=dim, tiled=True)  43.6 us
    all_to_all x1, starting transfers between devices, sent_to_all(): lax.all_to_all(jnp.broadcast_to(x[None], (size, *x.shape)), axis, 0, 0, t...  14.1 us
    all_to_all x1, starting transfers between devices, sum_at_owner(): pieces = lax.all_to_all(split_up(x, dim, size), axis, 0, 0, tiled=True)  14 us
    all_gather x1, blocking collectives, whole_of(): x = lax.all_gather(x, axis, axis=dim, tiled=True)  12 us
    all_to_all x1, waiting for transfers between devices, sum_at_owner(): pieces = lax.all_to_all(split_up(x, dim, size), axis, 0, 0, tiled=True)  9.23 us
  transfers between devices with their start and end apart: 8, of which 7 were waited for; matrix products, arithmetic and copies ran while one was open for 11% of the time, Pallas kernels for 0%

commit v1 on v0

v1 whole, which is shorter than its diff:
```python
import functools

import jax
import jax.numpy as jnp
from jax import lax
from jax.experimental import pallas as pl
from jax.experimental.pallas import tpu as pltpu
from jax.sharding import Mesh
from jax.sharding import PartitionSpec as P

GRID = 64
AXES = ("z", "y", "x", "c")
SP = ("z", "y")
TP = ("x", "c")
MESH_IDS = pl.DeviceIdType.MESH
F32 = jnp.float32
BF16 = jnp.bfloat16

epsilon = 1e-06
rope_base = 10000.0

NZ, NY, NX, NC = 16, 4, 4, 2
NT = NX * NC
PLANE = NY * NT
D = 2048
ROWS = 128
SHARE = 16
KEYS = NZ * NY * SHARE
QW = 256
KW = 384
WL = 640
UP = 384
TOK = 256


def rms_norm(values, gain):
    return (
        values * lax.rsqrt(jnp.mean(values * values, axis=-1, keepdims=True) + epsilon) * gain
    )


def rotate(values, positions):
    pair_count = values.shape[-1] // 4
    frequency = rope_base ** (-jnp.arange(pair_count, dtype=F32) / pair_count)
    grid_rows = (positions // GRID).astype(F32)
    grid_cols = (positions % GRID).astype(F32)
    angles = jnp.stack([grid_rows, grid_cols], axis=-1)[:, :, None] * frequency
    cosine = jnp.cos(angles)
    sine = jnp.sin(angles)
    halves = values.reshape(values.shape[:-1] + (2, 2, pair_count))
    leading = halves[..., 0, :]
    trailing = halves[..., 1, :]
    turned = jnp.stack(
        [leading * cosine - trailing * sine, trailing * cosine + leading * sine], axis=-2
    )
    return turned.reshape(values.shape)


def dot_nn(a, b):
    return jnp.dot(a, b, preferred_element_type=F32)


def dot_nt(a, b):
    return lax.dot_general(a, b, (((1,), (1,)), ((), ())), preferred_element_type=F32)


def layer_kernel(
    scale,
    kv_loc,
    q_loc,
    w_loc,
    ow,
    key_up,
    value_up,
    resid,
    gains,
    taps,
    out,
    kvbuf,
    qbuf,
    wbuf,
    owbuf,
    kvt,
    s_scr,
    ot_scr,
    stats,
    o_send,
    o_recv,
    r_send,
    r_recv,
    in_send,
    inbuf,
    up,
    p_send,
    p_recv,
    stream,
    kvs_z,
    kvs_y,
    kvr,
    qs,
    qr,
    wys,
    wyr,
    wzs,
    wps,
    wzr,
    wpr,
    ows,
    owr,
    sts,
    str_,
    os_,
    or_,
    rss,
    rsr,
    ags,
    agr,
    hs,
    hr,
    ps,
    pr,
):
    z, y, x, c = (lax.axis_index(a) for a in AXES)
    tp = x * NC + c
    plane = y * NT + tp
    half = y // 2

    def zz(k):
        return (z + k + NZ) % NZ

    def push(src, dst, ss, rs, dev):
        return pltpu.make_async_remote_copy(
            src_ref=src, dst_ref=dst, send_sem=ss, recv_sem=rs, device_id=dev,
            device_id_type=MESH_IDS,
        )

    partner = (z, y, x, 1 - c)
    right, left = (zz(1), y, x, c), (zz(-1), y, x, c)
    right2, left2 = (zz(2), y, x, c), (zz(-2), y, x, c)
    cross = ((z + 2 * c - 1 + NZ) % NZ, y, x, 1 - c)

    def on_plane(j):
        p = (plane + j) % PLANE
        return (z, p // NT, (p // NC) % NX, p % NC)

    def tp_peer(t):
        return (z, y, t // NC, t % NC)

    barrier = pltpu.get_barrier_semaphore()
    for dev in (right, left, right2, left2, cross):
        pl.semaphore_signal(barrier, inc=1, device_id=dev, device_id_type=MESH_IDS)

    @pl.loop(1, PLANE)
    def _(j):
        pl.semaphore_signal(barrier, inc=1, device_id=on_plane(j), device_id_type=MESH_IDS)

    def kv_slot(yy, k):
        start = pl.multiple_of((yy * NZ + k) * SHARE, SHARE)
        return kvbuf.at[pl.ds(start, SHARE)]

    def w_slot(core, k):
        return wbuf.at[core, pl.ds(pl.multiple_of(k * ROWS, ROWS), ROWS)]

    def w_part(k, yy):
        return wbuf.at[c, pl.ds(pl.multiple_of(k * ROWS + yy * 32, 32), 32)]

    kv_slot(y, z)[...] = kv_loc[...]
    qbuf[tp] = q_loc[...]
    w_part(z, y)[...] = w_loc[y]
    owbuf[c] = ow[...]

    pl.semaphore_wait(barrier, 5 + PLANE - 1)

    pending = []

    def go(copy):
        copy.start()
        pending.append(copy)

    def kv_to(k, sem, dev):
        slot = kv_slot(y, k)
        go(push(slot, slot, kvs_z.at[sem], kvr.at[y * NZ + k], dev))

    def kv_to_y(k, sem):
        slot = kv_slot(y, k)
        for j in range(1, NY):
            dev = (z, (y + j) % NY, x, c)
            go(push(slot, slot, kvs_y.at[sem * 3 + j - 1], kvr.at[y * NZ + k], dev))

    kv_to(z, 0, right2)
    kv_to(z, 1, left2)
    kv_to(z, 2, right)
    kv_to(z, 3, left)
    kv_to_y(z, 0)
    for j in range(1, NY):
        yy = (y + j) % NY
        go(push(w_loc.at[yy], w_part(z, y), wys.at[j - 1], wyr.at[y], (z, yy, x, c)))
    for j in range(1, NT):
        t = (tp + j) % NT
        go(push(qbuf.at[tp], qbuf.at[tp], qs.at[j - 1], qr.at[tp], tp_peer(t)))
    go(push(owbuf.at[c], owbuf.at[c], ows.at[0], owr.at[0], partner))

    def w_send(k, step, to_right, to_left):
        slot = w_slot(c, k)
        if to_right:
            go(push(slot, slot, wzs.at[step], wzr.at[k], right))
        if to_left:
            go(push(slot, slot, wzs.at[8 + step], wzr.at[k], left))

    def w_across(k, sem):
        slot = w_slot(c, k)
        go(push(slot, slot, wps.at[sem], wpr.at[k], partner))

    def w_step(step):
        if step == 0:
            for j in range(1, NY):
                yy = (y + j) % NY
                part = w_part(z, yy)
                push(part, part, wys.at[j - 1], wyr.at[yy], (z, yy, x, c)).wait_recv()
            w_send(z, 0, True, True)
            w_across(z, 0)
            return
        k = zz(-step)
        slot = w_slot(c, k)
        push(slot, slot, wzs.at[0], wzr.at[k], left).wait_recv()
        w_send(k, step, step < 8, False)
        w_across(k, 2 * step - 1)
        if step < 8:
            k = zz(step)
            slot = w_slot(c, k)
            push(slot, slot, wzs.at[0], wzr.at[k], right).wait_recv()
            w_send(k, step, False, step < 7)
            w_across(k, 2 * step)

    def kv_wait(yy, k):
        slot = kv_slot(yy, k)
        push(slot, slot, kvs_z.at[0], kvr.at[yy * NZ + k], right).wait_recv()

    for d in range(1, 9):
        k = zz(-d)
        kv_wait(y, k)
        if d + 2 <= 8:
            kv_to(k, 3 + d, right2)
        if d < 8:
            k2 = zz(d)
            kv_wait(y, k2)
            if d + 2 <= 7:
                kv_to(k2, 9 + d, left2)
        kv_to_y(k, 2 * d - 1)
        if d < 8:
            kv_to_y(k2, 2 * d)
        if d == 3:
            w_step(0)
    for j in range(1, NY):
        yy = (y + j) % NY

        @pl.loop(0, NZ)
        def _(k):
            kv_wait(yy, k)

    w_step(1)
    for j in range(1, NT):
        t = (tp + j) % NT
        push(qbuf.at[t], qbuf.at[t], qs.at[0], qr.at[t], tp_peer(t)).wait_recv()

    kvt[...] = kvbuf[:, :256].T
    for hp in range(4):
        pair = []
        for h in (2 * hp, 2 * hp + 1):
            folded = dot_nt(qbuf[h, :, :128], key_up[:, h * 128 : (h + 1) * 128])
            pair.append(jnp.concatenate([folded.astype(BF16), qbuf[h, :, 128:]], axis=1))
        q = jnp.concatenate(pair, axis=0)
        s_scr[...] = dot_nt(kvbuf[...], q)
        top = jnp.max(s_scr[...], axis=0, keepdims=True)
        weights = jnp.exp((s_scr[...] - top) * scale)
        total = jnp.sum(weights, axis=0, keepdims=True)
        ot_scr[hp] = dot_nn(kvt[...], weights.astype(BF16))
        for i in range(2):
            h = 2 * hp + i
            stats[tp, h : h + 1] = top[:, i * 128 : (i + 1) * 128]
            stats[tp, 8 + h : 9 + h] = total[:, i * 128 : (i + 1) * 128]
        if hp == 2:
            w_step(2)

    for j in range(1, NT):
        t = (tp + j) % NT
        go(push(stats.at[tp], stats.at[tp], sts.at[j - 1], str_.at[tp], tp_peer(t)))
    for j in range(1, NT):
        t = (tp + j) % NT
        push(stats.at[t], stats.at[t], sts.at[0], str_.at[t], tp_peer(t)).wait_recv()
    top_all = stats[0, 0:8]
    for t in range(1, NT):
        top_all = jnp.maximum(top_all, stats[t, 0:8])
    total_all = jnp.zeros_like(top_all)
    for t in range(NT):
        total_all += jnp.exp((stats[t, 0:8] - top_all) * scale) * stats[t, 8:16]
    factor = jnp.exp((stats[tp, 0:8] - top_all) * scale) / total_all
    for hp in range(4):
        for i in range(2):
            h = 2 * hp + i
            turned = ot_scr[hp, :, i * 128 : (i + 1) * 128] * factor[h : h + 1]
            mixed = dot_nn(turned.T.astype(BF16), value_up[:, h * 128 : (h + 1) * 128])
            blocks = mixed.astype(BF16).reshape(NX, NC, SHARE, 128)
            for core in range(NC):
                o_send[hp * NC + core, i * 64 : (i + 1) * 64] = blocks[:, core].reshape(64, 128)
    for j in range(1, NT):
        t = (tp + j) % NT
        go(push(o_send.at[t], o_recv.at[tp], os_.at[j - 1], or_.at[tp], tp_peer(t)))
    o_recv[tp] = o_send[tp]
    w_step(3)
    push(owbuf.at[1 - c], owbuf.at[1 - c], ows.at[0], owr.at[0], partner).wait_recv()
    for j in range(1, NT):
        t = (tp + j) % NT
        push(o_recv.at[t], o_recv.at[t], os_.at[0], or_.at[t], tp_peer(t)).wait_recv()
    attended = o_recv[0].astype(F32)
    for t in range(1, NT):
        attended += o_recv[t].astype(F32)
    attended = attended.astype(BF16)
    r_send[...] = (
        dot_nn(attended[:64], owbuf[0]) + dot_nn(attended[64:], owbuf[1])
    ).astype(BF16)
    for j in range(1, NX):
        xx = (x + j) % NX
        src = r_send.at[pl.ds(pl.multiple_of(xx * SHARE, SHARE), SHARE)]
        go(push(src, r_recv.at[x], rss.at[j - 1], rsr.at[x], (z, y, xx, c)))
    r_recv[x] = r_send[pl.ds(pl.multiple_of(x * SHARE, SHARE), SHARE)]
    for j in range(1, NX):
        xx = (x + j) % NX
        push(r_recv.at[xx], r_recv.at[xx], rss.at[0], rsr.at[xx], (z, y, xx, c)).wait_recv()
    summed = r_recv[0].astype(F32)
    for j in range(1, NX):
        summed += r_recv[j].astype(F32)
    summed = summed.astype(BF16).astype(F32)
    flow = (resid[...].astype(F32) + rms_norm(summed, gains[0:1])).astype(BF16).astype(F32)
    stream[...] = flow
    in_send[...] = rms_norm(flow, gains[1:2]).astype(BF16)

    def in_slot(s):
        return inbuf.at[pl.ds(pl.multiple_of(s * SHARE, SHARE), SHARE)]

    mine = (y % 2) * NT + tp

    def ag_copy(j):
        chip = (y * NX + x + j) % (NY * NX)
        dev = (z, chip // NX, chip % NX, half)
        return push(in_send, in_slot(mine), ags.at[j], agr.at[mine], dev)

    @pl.loop(1, NY * NX)
    def _(j):
        ag_copy(j).start()

    @pl.when(half == c)
    def _():
        in_slot(mine)[...] = in_send[...]

    @pl.when(half != c)
    def _():
        ag_copy(0).start()

    for step in range(4, 9):
        w_step(step)

    @pl.loop(0, NZ)
    def _(k):
        slot = w_slot(1 - c, k)
        push(slot, slot, wps.at[0], wpr.at[k], partner).wait_recv()

    own_slot = jnp.where(half == c, mine, -1)

    @pl.loop(0, 16)
    def _(s):
        @pl.when(s != own_slot)
        def _():
            push(in_slot(s), in_slot(s), ags.at[0], agr.at[s], partner).wait_recv()

    for core in range(NC):
        up[core, 8 : 8 + TOK] = dot_nn(inbuf[...], wbuf[core, :, :UP])

    low_dev = ((z + c) % NZ, y, x, 1 - c)
    high_dev = ((z + c - 1 + NZ) % NZ, y, x, 1 - c)
    go(push(up.at[:, pl.ds(TOK, 8)], up.at[:, pl.ds(0, 8)], hs.at[0], hr.at[0], low_dev))
    go(push(up.at[:, pl.ds(8, 8)], up.at[:, pl.ds(TOK + 8, 8)], hs.at[1], hr.at[1], high_dev))
    low, high = up.at[:, pl.ds(0, 8)], up.at[:, pl.ds(TOK + 8, 8)]
    push(low, low, hs.at[0], hr.at[0], low_dev).wait_recv()
    push(high, high, hs.at[1], hr.at[1], high_dev).wait_recv()

    @pl.when((z == 0) & (c == 0))
    def _():
        up[:, 0:8] = jnp.zeros((NC, 8, UP), F32)

    @pl.when((z == NZ - 1) & (c == 1))
    def _():
        up[:, TOK + 8 : TOK + 16] = jnp.zeros((NC, 8, UP), F32)

    hidden = []
    for core in range(NC):
        conv = (
            up[core, 7 : 7 + TOK] * taps[core, 0:1]
            + up[core, 8 : 8 + TOK] * taps[core, 1:2]
            + up[core, 9 : 9 + TOK] * taps[core, 2:3]
        )
        gate = conv[:, 128:256]
        first = gate / (1.0 + jnp.exp(-gate)) * conv[:, :128]
        gate = pltpu.roll(conv[:, 256:], 64, 1)
        second = gate / (1.0 + jnp.exp(-gate)) * conv[:, 256:]
        lane = lax.broadcasted_iota(jnp.int32, second.shape, 1)
        second = jnp.where(lane < 64, second, 0.0)
        hidden.append(jnp.concatenate([first.astype(BF16), second.astype(BF16)], axis=1))
    p_send[...] = (
        dot_nt(hidden[0], wbuf[0, :, UP:]) + dot_nt(hidden[1], wbuf[1, :, UP:])
    ).astype(BF16)

    chip = y * NX + x

    def p_slot(s):
        return p_send.at[pl.ds(pl.multiple_of(s * SHARE, SHARE), SHARE)]

    def rs_copy(s):
        dev = (z, 2 * c + s // NT, (s // NC) % NX, s % NC)
        return push(p_slot(s), p_recv.at[chip], ps.at[s], pr.at[chip], dev)

    @pl.loop(0, 16)
    def _(j):
        s = (mine + j) % 16

        @pl.when(s != own_slot)
        def _():
            rs_copy(s).start()

    @pl.when(half == c)
    def _():
        p_recv[chip] = p_slot(mine)[...]

    own_chip = jnp.where(half == c, chip, -1)

    @pl.loop(0, 16)
    def _(k):
        @pl.when(k != own_chip)
        def _():
            push(p_recv.at[k], p_recv.at[k], ps.at[0], pr.at[k], partner).wait_recv()

    projected = p_recv[0].astype(F32)
    for k in range(1, 16):
        projected += p_recv[k].astype(F32)
    projected = projected.astype(BF16).astype(F32)
    out[...] = (stream[...] + rms_norm(projected, gains[2:3])).astype(BF16)

    for copy in pending:
        copy.wait_send()

    @pl.loop(1, NY * NX)
    def _(j):
        ag_copy(j).wait_send()

    @pl.when(half != c)
    def _():
        ag_copy(0).wait_send()

    @pl.loop(0, 16)
    def _(s):
        @pl.when(s != own_slot)
        def _():
            rs_copy(s).wait_send()


def body(
    residual,
    query_nope,
    query_rope,
    latent,
    rope_key,
    kv_gain,
    key_up,
    value_up,
    out_weight,
    post_gain,
    pre_gain,
    ffn_gain,
    up_value,
    up_gate,
    conv_value,
    conv_gate,
    down_weight,
):
    tp = lax.axis_index(TP)
    y = lax.axis_index("y")
    sp = lax.axis_index(SP)
    scale = (query_nope.shape[2] + query_rope.shape[2]) ** (-0.5)
    positions = sp * ROWS + jnp.arange(ROWS, dtype=jnp.int32)
    key_positions = sp * ROWS + tp * SHARE + jnp.arange(SHARE, dtype=jnp.int32)

    def own_rows(a):
        return lax.dynamic_slice_in_dim(a, tp * SHARE, SHARE, 0)

    normed = rms_norm(own_rows(latent).astype(F32), kv_gain.astype(F32)).astype(BF16)
    key_turn = rotate(own_rows(rope_key).astype(F32), key_positions).astype(BF16)
    query_turn = rotate(query_rope[:, 0].astype(F32), positions).astype(BF16)
    kv_loc = jnp.concatenate([normed, key_turn, jnp.zeros((SHARE, 64), BF16)], axis=1)
    q_loc = jnp.concatenate([query_nope[:, 0], query_turn, jnp.zeros((ROWS, 64), BF16)], axis=1)

    width = up_value.shape[1] // NY
    rest = width - 128

    def by_y(a):
        return jnp.transpose(a.reshape(a.shape[0], NY, width), (1, 0, 2))

    def lanes(v, g):
        pad = jnp.zeros(v.shape[:-1] + (64 - rest,), v.dtype)
        return [v[..., :128], g[..., :128], v[..., 128:], pad, g[..., 128:], pad]

    value, gate, down = by_y(up_value), by_y(up_gate), by_y(down_weight.T)
    w_loc = jnp.concatenate(
        lanes(value, gate) + [down, jnp.zeros(down.shape[:-1] + (256 - width,), BF16)], axis=-1
    )

    def chip_taps(core):
        start = (tp // NC * NC + core) * width * NY + y * width
        v = lax.dynamic_slice_in_dim(conv_value, start, width, 1)
        g = lax.dynamic_slice_in_dim(conv_gate, start, width, 1)
        return jnp.concatenate(lanes(v, g), axis=-1)

    taps = jnp.stack([chip_taps(0), chip_taps(1)]).astype(F32)
    taps = jnp.pad(taps, ((0, 0), (0, 5), (0, 0)))
    gains = jnp.pad(jnp.stack([post_gain, pre_gain, ffn_gain]).astype(F32), ((0, 5), (0, 0)))

    dma = pltpu.SemaphoreType.DMA
    vmem = pltpu.VMEM
    return pl.pallas_call(
        functools.partial(layer_kernel, scale),
        out_shape=jax.ShapeDtypeStruct((SHARE, D), BF16),
        in_specs=[pl.BlockSpec(memory_space=vmem)] * 9,
        out_specs=pl.BlockSpec(memory_space=vmem),
        scratch_shapes=[
            vmem((KEYS, KW), BF16),
            vmem((NT, ROWS, QW), BF16),
            vmem((NC, NZ * ROWS, WL), BF16),
            vmem((NC, 128, D), BF16),
            vmem((256, KEYS), BF16),
            vmem((KEYS, 256), F32),
            vmem((4, 256, 256), F32),
            vmem((NT, 16, 128), F32),
            vmem((NT, 128, 128), BF16),
            vmem((NT, 128, 128), BF16),
            vmem((64, D), BF16),
            vmem((NX, SHARE, D), BF16),
            vmem((SHARE, D), BF16),
            vmem((TOK, D), BF16),
            vmem((NC, TOK + 16, UP), F32),
            vmem((TOK, D), BF16),
            vmem((NY * NX, SHARE, D), BF16),
            vmem((SHARE, D), F32),
        ]
        + [
            dma((n,))
            for n in (15, 48, 64, 7, 8, 3, 4, 16, 16, 16, 16, 1, 1, 7, 8, 7, 8, 3, 4, 16, 16, 2, 2, 16, 16)
        ],
        compiler_params=pltpu.CompilerParams(
            collective_id=0, has_side_effects=True, vmem_limit_bytes=60 * 1024 * 1024
        ),
        name="layer",
    )(
        kv_loc,
        q_loc,
        w_loc,
        out_weight,
        key_up.reshape(key_up.shape[0], -1),
        value_up.reshape(value_up.shape[0], -1),
        own_rows(residual),
        gains,
        taps,
    )


def solution(mesh):
    torus = Mesh(mesh.devices.reshape(NZ, NY, NX, NC), AXES)
    return jax.shard_map(
        body,
        mesh=torus,
        in_specs=(
            P(SP, None),
            P(SP, TP, None),
            P(SP, TP, None),
            P(SP, None),
            P(SP, None),
            P(),
            P(),
            P(),
            P(TP, None),
            P(),
            P(),
            P(),
            P(SP, TP),
            P(SP, TP),
            P(),
            P(),
            P(TP, SP),
        ),
        out_specs=P(SP + TP, None),
        check_vma=False,
    )
```

time: 409 us -> 122 us (0.30)
  waiting for transfers between devices: 300 us -> 0 us
  Pallas kernels: 0 us -> 107 us
  starting transfers between devices: 32 us -> 0 us
  matrix products: 25.3 us -> 0 us
  between operations: 13.4 us -> 0.27 us
  blocking collectives: 12 us -> 0 us
  other arithmetic: 15 us -> 4.52 us
    all_gather x4 -> x0, waiting for transfers between devices: 283 us -> none  [the longest x1 150 us: side_by_side(): whole, at, outs = (lax.all_gather(both, axis, axis=dim, tiled=True), 0, [])]
    pallas_call x0 -> x1, Pallas kernels: none -> 107 us  [body(): pl.pallas_call(functools.partial(layer_kernel, scale), out_shape=jax.Shap...]
    all_to_all x2 -> x0, starting transfers between devices: 28.1 us -> none  [the longest x1 14.1 us: sent_to_all(): lax.all_to_all(jnp.broadcast_to(x[None], (size, *x.shape)), axis, 0, 0, t...]
    dot_general x6 -> x0, matrix products: 25.3 us -> none  [the longest x1 7.59 us: body(): jnp.einsum('qhd,khd->hqk', query_nope, keys_nope, preferred_element_type=...]
    all_to_all x2 -> x0, waiting for transfers between devices: 14 us -> none  [the longest x1 9.23 us: sum_at_owner(): pieces = lax.all_to_all(split_up(x, dim, size), axis, 0, 0, tiled=True)]
    all_gather x1 -> x0, blocking collectives: 12 us -> none  [whole_of(): x = lax.all_gather(x, axis, axis=dim, tiled=True)]
    reduce_sum x3 -> x0, other arithmetic: 6.32 us -> none  [the longest x1 3.29 us: body(): totals = jnp.sum(weights, axis=-1)]
    transpose x1 -> x0, local copies, waits for them, and re-layouts: 5.83 us -> none  [stacked_from(): pieces.transpose(*turned, *range(len(order), pieces.ndim))]
  transfers between devices with their start and end apart: 8 -> 0, of which waited for: 7 -> 0; matrix products, arithmetic and copies ran while one was open for 11% -> 0% of each run, Pallas kernels for 0% -> 0%
where the time goes in v1:
time: 122 us; the launch traced here: 121 us
  Pallas kernels  107 us (88%)
  local copies, waits for them, and re-layouts  10 us (8%)
  other arithmetic  4.52 us (4%)
    pallas_call x1, Pallas kernels, body(): pl.pallas_call(functools.partial(layer_kernel, scale), out_shape=jax.Shap...  107 us
    unnamed x29, local copies, waits for them, and re-layouts  4.68 us

profile of v1, /device:TPU:1, one launch (start us, length us, event | category | flops | bytes accessed | tf_op | source)
XLA Modules:
  0.0 121.3 jit_solution(3450099995021254373)
XLA Ops:
  0.0 0.0 copy-start
  0.0 0.1 pad.23.clone
  0.1 0.1 pad.30.clone
  0.2 0.8 fusion.16
  1.1 0.0 copy-start.12
  1.1 0.6 copy-done.12
  1.7 0.8 constant_dynamic-slice_fusion.2
  2.5 0.8 constant_dynamic-slice_fusion.6
  3.3 0.1 concatenate.18
  3.4 0.1 concatenate.19
  3.5 0.0 copy-start.9
  3.5 0.0 copy-start.10
  3.5 0.8 fusion.18
  4.3 0.0 copy-done.9
  4.3 0.0 copy-start.8
  4.3 0.0 copy-done.10
  4.4 0.0 copy-start.11
  4.4 0.7 copy-done.11
  5.1 0.0 copy-done.8
  5.1 0.1 constant_dynamic-slice_fusion.9
  5.2 0.1 copy.51
  5.2 0.1 copy.50
  5.3 0.1 fusion.24
  5.5 0.1 convert_element_type.76
  5.6 0.6 maximum_maximum_fusion.1.kv_loc
  6.2 0.0 copy-start.7
  6.2 0.6 fusion.28.taps
  6.8 0.1 copy-done.7
  6.9 0.1 fusion.20
  7.1 0.0 copy-start.6
  7.1 0.1 copy.44
  7.2 0.6 copy-done.6
  7.8 0.6 maximum_maximum_fusion.q_loc
  8.5 0.7 fusion.5.gains
  9.1 0.0 copy-done
  9.1 0.0 copy-start.3
  9.1 0.6 constant_dynamic-slice_fusion.8.resid
  9.8 0.2 copy-done.3
  9.9 0.1 reshape.222
  10.1 0.0 copy-start.4
  10.1 0.0 copy-start.5
  10.1 0.8 copy-done.4
  10.9 0.0 copy-start.2
  10.9 0.1 reshape.223
  11.0 0.0 copy-start.1
  11.1 0.0 copy-done.5
  11.1 0.1 reshape.224
  11.2 0.8 concatenate.17.w_loc
  12.0 0.0 copy-done.2
  12.0 0.1 copy-done.1
  12.1 1.2 copy_bitcast_fusion
  13.3 106.5 %layer.1 = bf16[16,2048]{1,0:T(8,128)(2,1)} custom-call(bf16[16,384]{1,0:T(8,128)(2,1)} %maximum_maximum_fusion.1.kv_loc, bf16[128,256]{1,0:T(8,128)(2,1)} %maximum_maximum_fusion.q_loc, bf16[4,32,640]{2,1,0:T(8,128)(2,1)} %concatenate.17.w_loc, bf16[128,2048]{1,0:T(8,128)(2,1)} %ow.1, bf16[256,1024]{1,0:T(8,128)(2,1)} %get-tuple-element.28.key_up, ...), custom_call_target="tpu_custom_call" | custom-call | tf_op jit(solution)/shard_map/layer/pallas_call | solution.py:528
  119.9 1.5 %copy.63 = bf16[16,2048]{1,0:T(8,128)(2,1)} copy(bf16[16,2048]{1,0:T(8,128)(2,1)} %layer.1) | data formatting | bytes 131072
  (26 shorter events, 0.2 us)
Async XLA Ops:
  0.0 9.1 %copy-start = (bf16[128,2048]{1,0:T(8,128)(2,1)S(1)}, bf16[128,2048]{1,0:T(8,128)(2,1)}, u32[]{:S(2)}) copy-start(bf16[128,2048]{1,0:T(8,128)(2,1)} %param.17) | copy-start | bytes 1572868
  1.1 0.7 copy-start.12
  3.5 0.8 copy-start.9
  3.5 0.8 copy-start.10
  4.3 0.7 copy-start.8
  4.4 0.7 copy-start.11
  6.2 0.7 copy-start.7
  7.1 0.8 copy-start.6
  9.1 0.8 copy-start.3
  10.1 0.8 copy-start.4
  10.1 1.0 copy-start.5
  10.9 1.2 copy-start.2
  11.0 1.1 copy-start.1

commit v2 on v1

--- a/solution.py
+++ b/solution.py
@@ -2,6 +2,7 @@
 
 import jax
 import jax.numpy as jnp
+import numpy as np
 from jax import lax
 from jax.experimental import pallas as pl
 from jax.experimental.pallas import tpu as pltpu
@@ -30,6 +31,8 @@
 KW = 384
 WL = 640
 UP = 384
+HID = 176
+W_AT = {1: 0, 5: 1, 8: 2}
 TOK = 256
 
 
@@ -39,21 +42,32 @@
     )
 
 
-def rotate(values, positions):
-    pair_count = values.shape[-1] // 4
-    frequency = rope_base ** (-jnp.arange(pair_count, dtype=F32) / pair_count)
-    grid_rows = (positions // GRID).astype(F32)
-    grid_cols = (positions % GRID).astype(F32)
-    angles = jnp.stack([grid_rows, grid_cols], axis=-1)[:, :, None] * frequency
-    cosine = jnp.cos(angles)
-    sine = jnp.sin(angles)
-    halves = values.reshape(values.shape[:-1] + (2, 2, pair_count))
-    leading = halves[..., 0, :]
-    trailing = halves[..., 1, :]
-    turned = jnp.stack(
-        [leading * cosine - trailing * sine, trailing * cosine + leading * sine], axis=-2
-    )
-    return turned.reshape(values.shape)
+def turn_tables():
+    pairs = 16
+    frequency = rope_base ** (-np.arange(pairs) / pairs)
+    sign = np.repeat([-1.0, 1.0], pairs)
+
+    def both(steps, at):
+        angles = np.tile(np.arange(steps)[:, None] * frequency, (1, 2))
+        table = np.zeros((2, steps, 128))
+        table[0, :, at : at + 32] = np.cos(angles)
+        table[1, :, at : at + 32] = np.sin(angles) * sign
+        return table
+
+    by_row = both(ROWS // GRID * NZ * NY, 0).reshape(2, NZ * NY, ROWS // GRID, 128)
+    by_row = by_row.transpose(1, 0, 2, 3).reshape(NZ * NY, 2 * ROWS // GRID, 128)
+    by_row = np.pad(by_row, ((0, 0), (0, 8 - 2 * ROWS // GRID), (0, 0)))
+    return by_row.astype(np.float32), both(GRID, 32).astype(np.float32)
+
+
+def turned(values, cosine, sine):
+    lane = lax.broadcasted_iota(jnp.int32, values.shape, 1)
+    other = jnp.where((lane & 16) == 0, pltpu.roll(values, 112, 1), pltpu.roll(values, 16, 1))
+    return values * cosine + other * sine
+
+
+def widen64(values):
+    return jnp.concatenate([values.astype(F32), jnp.zeros(values.shape, F32)], axis=1)
 
 
 def dot_nn(a, b):
@@ -64,17 +78,33 @@
     return lax.dot_general(a, b, (((1,), (1,)), ((), ())), preferred_element_type=F32)
 
 
+def side_lanes(v, g):
+    rest = HID - 128
+    pad = jnp.zeros(v.shape[:-1] + (64 - rest,), v.dtype)
+    return [v[:, :128], g[:, :128], v[:, 128:], pad, g[:, 128:], pad]
+
+
 def layer_kernel(
     scale,
-    kv_loc,
-    q_loc,
-    w_loc,
+    latent,
+    rope_key,
+    kv_gain,
+    q_nope,
+    q_rope,
+    by_row,
+    by_col,
+    up_value,
+    up_gate,
+    down,
     ow,
     key_up,
     value_up,
     resid,
-    gains,
-    taps,
+    post_gain,
+    pre_gain,
+    ffn_gain,
+    conv_value,
+    conv_gate,
     out,
     kvbuf,
     qbuf,
@@ -94,6 +124,28 @@
     p_send,
     p_recv,
     stream,
+    latent_v,
+    rope_key_v,
+    kv_gain_v,
+    q_nope_v,
+    q_rope_v,
+    by_row_v,
+    by_col_v,
+    up_value_v,
+    up_gate_v,
+    down_v,
+    key_up_v,
+    value_up_v,
+    resid_v,
+    gains,
+    conv_v,
+    turns,
+    w_loc,
+    wide,
+    qf,
+    vu,
+    taps,
+    loads,
     kvs_z,
     kvs_y,
     kvr,
@@ -146,6 +198,39 @@
     def tp_peer(t):
         return (z, y, t // NC, t % NC)
 
+    def own(ref):
+        return ref.at[pl.ds(pl.multiple_of(tp * SHARE, SHARE), SHARE)]
+
+    local = {}
+
+    def load(name, src, dst):
+        local[name] = pltpu.make_async_copy(src, dst, loads.at[len(local)])
+        local[name].start()
+
+    load("latent", own(latent), latent_v)
+    load("rope_key", own(rope_key), rope_key_v)
+    load("by_row", by_row.at[z * NY + y], by_row_v)
+    load("by_col", by_col, by_col_v)
+    load("kv_gain", kv_gain, kv_gain_v)
+    load("q_nope", q_nope, q_nope_v)
+    load("q_rope", q_rope, q_rope_v)
+    load("up_value", up_value, up_value_v)
+    load("up_gate", up_gate, up_gate_v)
+    load("down", down, down_v)
+    load("ow", ow, owbuf.at[c])
+    load("key_up", key_up, key_up_v)
+    load("value_up", value_up, value_up_v)
+    load("resid", own(resid), resid_v)
+    load("post", post_gain, gains.at[0])
+    load("pre", pre_gain, gains.at[1])
+    load("ffn", ffn_gain, gains.at[2])
+    load("conv_value", conv_value, conv_v.at[0])
+    load("conv_gate", conv_gate, conv_v.at[1])
+
+    def ready(*names):
+        for name in names:
+            local[name].wait()
+
     barrier = pltpu.get_barrier_semaphore()
     for dev in (right, left, right2, left2, cross):
         pl.semaphore_signal(barrier, inc=1, device_id=dev, device_id_type=MESH_IDS)
@@ -164,10 +249,19 @@
     def w_part(k, yy):
         return wbuf.at[c, pl.ds(pl.multiple_of(k * ROWS + yy * 32, 32), 32)]
 
-    kv_slot(y, z)[...] = kv_loc[...]
-    qbuf[tp] = q_loc[...]
-    w_part(z, y)[...] = w_loc[y]
-    owbuf[c] = ow[...]
+    ready("latent", "rope_key", "by_row", "by_col", "kv_gain")
+    for i in range(2):
+        grid_rows = [
+            by_row_v[2 * i + j : 2 * i + j + 1] + by_col_v[i] for j in range(ROWS // GRID)
+        ]
+        turns[i] = jnp.concatenate(grid_rows, axis=0)
+    rows = pl.ds(pl.multiple_of(tp * SHARE, SHARE), SHARE)
+    kv_slot(y, z)[:, :256] = rms_norm(
+        latent_v[...].astype(F32), kv_gain_v[...].astype(F32)
+    ).astype(BF16)
+    kv_slot(y, z)[:, 256:] = turned(
+        widen64(rope_key_v[...]), turns[0, rows], turns[1, rows]
+    ).astype(BF16)
 
     pl.semaphore_wait(barrier, 5 + PLANE - 1)
 
@@ -192,12 +286,29 @@
     kv_to(z, 2, right)
     kv_to(z, 3, left)
     kv_to_y(z, 0)
+    ready("q_nope", "q_rope")
+    qbuf[tp, :, :128] = q_nope_v[...]
+    qbuf[tp, :, 128:] = turned(widen64(q_rope_v[...]), turns[0], turns[1]).astype(BF16)
+    for j in range(1, NT):
+        t = (tp + j) % NT
+        go(push(qbuf.at[tp], qbuf.at[tp], qs.at[j - 1], qr.at[tp], tp_peer(t)))
+
+    ready("up_value", "up_gate", "down")
+    eye = (
+        lax.broadcasted_iota(jnp.int32, (32, 32), 0) == lax.broadcasted_iota(jnp.int32, (32, 32), 1)
+    ).astype(BF16)
+    value, gate = up_value_v[...].astype(F32), up_gate_v[...].astype(F32)
+    across = dot_nt(eye, down_v[...])
+    for yy in range(NY):
+        at = slice(yy * HID, (yy + 1) * HID)
+        parts = side_lanes(value[:, at], gate[:, at])
+        parts += [across[:, at], jnp.zeros((32, 256 - HID), F32)]
+        w_loc[yy] = jnp.concatenate(parts, axis=1).astype(BF16)
     for j in range(1, NY):
         yy = (y + j) % NY
         go(push(w_loc.at[yy], w_part(z, y), wys.at[j - 1], wyr.at[y], (z, yy, x, c)))
-    for j in range(1, NT):
-        t = (tp + j) % NT
-        go(push(qbuf.at[tp], qbuf.at[tp], qs.at[j - 1], qr.at[tp], tp_peer(t)))
+    w_part(z, y)[...] = w_loc[y]
+    ready("ow")
     go(push(owbuf.at[c], owbuf.at[c], ows.at[0], owr.at[0], partner))
 
     def w_send(k, step, to_right, to_left):
@@ -236,7 +347,29 @@
         slot = kv_slot(yy, k)
         push(slot, slot, kvs_z.at[0], kvr.at[yy * NZ + k], right).wait_recv()
 
+    def fold_queries():
+        for j in range(1, NT):
+            t = (tp + j) % NT
+            push(qbuf.at[t], qbuf.at[t], qs.at[0], qr.at[t], tp_peer(t)).wait_recv()
+        ready("key_up")
+        wide[...] = key_up_v[...].astype(F32)
+        for h in range(NT):
+            up_h = wide[pl.ds(h, 256, stride=NT)].astype(BF16)
+            r = slice(h % 2 * 128, h % 2 * 128 + 128)
+            qf[h // 2, r, :256] = dot_nt(qbuf[h, :, :128], up_h).astype(BF16)
+            qf[h // 2, r, 256:] = qbuf[h, :, 128:]
+
+    def split_values():
+        ready("value_up")
+        wide[...] = value_up_v[...].astype(F32)
+        for h in range(NT):
+            vu[h] = wide[pl.ds(h, 256, stride=NT)].astype(BF16)
+
     for d in range(1, 9):
+        if d == 4:
+            fold_queries()
+        if d == 6:
+            split_values()
         k = zz(-d)
         kv_wait(y, k)
         if d + 2 <= 8:
@@ -249,8 +382,8 @@
         kv_to_y(k, 2 * d - 1)
         if d < 8:
             kv_to_y(k2, 2 * d)
-        if d == 3:
-            w_step(0)
+        if d in W_AT:
+            w_step(W_AT[d])
     for j in range(1, NY):
         yy = (y + j) % NY
 
@@ -258,33 +391,25 @@
         def _(k):
             kv_wait(yy, k)
 
-    w_step(1)
-    for j in range(1, NT):
-        t = (tp + j) % NT
-        push(qbuf.at[t], qbuf.at[t], qs.at[0], qr.at[t], tp_peer(t)).wait_recv()
-
     kvt[...] = kvbuf[:, :256].T
     for hp in range(4):
-        pair = []
-        for h in (2 * hp, 2 * hp + 1):
-            folded = dot_nt(qbuf[h, :, :128], key_up[:, h * 128 : (h + 1) * 128])
-            pair.append(jnp.concatenate([folded.astype(BF16), qbuf[h, :, 128:]], axis=1))
-        q = jnp.concatenate(pair, axis=0)
-        s_scr[...] = dot_nt(kvbuf[...], q)
-        top = jnp.max(s_scr[...], axis=0, keepdims=True)
-        weights = jnp.exp((s_scr[...] - top) * scale)
+        s_now = s_scr.at[hp % 2]
+        s_now[...] = dot_nt(kvbuf[...], qf[hp])
+        top = jnp.max(s_now[...], axis=0, keepdims=True)
+        weights = jnp.exp((s_now[...] - top) * scale)
         total = jnp.sum(weights, axis=0, keepdims=True)
         ot_scr[hp] = dot_nn(kvt[...], weights.astype(BF16))
         for i in range(2):
             h = 2 * hp + i
             stats[tp, h : h + 1] = top[:, i * 128 : (i + 1) * 128]
             stats[tp, 8 + h : 9 + h] = total[:, i * 128 : (i + 1) * 128]
-        if hp == 2:
-            w_step(2)
+        if hp == 1:
+            w_step(3)
 
     for j in range(1, NT):
         t = (tp + j) % NT
         go(push(stats.at[tp], stats.at[tp], sts.at[j - 1], str_.at[tp], tp_peer(t)))
+    w_step(4)
     for j in range(1, NT):
         t = (tp + j) % NT
         push(stats.at[t], stats.at[t], sts.at[0], str_.at[t], tp_peer(t)).wait_recv()
@@ -298,8 +423,8 @@
     for hp in range(4):
         for i in range(2):
             h = 2 * hp + i
-            turned = ot_scr[hp, :, i * 128 : (i + 1) * 128] * factor[h : h + 1]
-            mixed = dot_nn(turned.T.astype(BF16), value_up[:, h * 128 : (h + 1) * 128])
+            scaled = ot_scr[hp, :, i * 128 : (i + 1) * 128] * factor[h : h + 1]
+            mixed = dot_nn(scaled.T.astype(BF16), vu[h])
             blocks = mixed.astype(BF16).reshape(NX, NC, SHARE, 128)
             for core in range(NC):
                 o_send[hp * NC + core, i * 64 : (i + 1) * 64] = blocks[:, core].reshape(64, 128)
@@ -307,7 +432,7 @@
         t = (tp + j) % NT
         go(push(o_send.at[t], o_recv.at[tp], os_.at[j - 1], or_.at[tp], tp_peer(t)))
     o_recv[tp] = o_send[tp]
-    w_step(3)
+    w_step(5)
     push(owbuf.at[1 - c], owbuf.at[1 - c], ows.at[0], owr.at[0], partner).wait_recv()
     for j in range(1, NT):
         t = (tp + j) % NT
@@ -327,13 +452,14 @@
     for j in range(1, NX):
         xx = (x + j) % NX
         push(r_recv.at[xx], r_recv.at[xx], rss.at[0], rsr.at[xx], (z, y, xx, c)).wait_recv()
+    ready("resid", "post", "pre", "ffn")
     summed = r_recv[0].astype(F32)
     for j in range(1, NX):
         summed += r_recv[j].astype(F32)
     summed = summed.astype(BF16).astype(F32)
-    flow = (resid[...].astype(F32) + rms_norm(summed, gains[0:1])).astype(BF16).astype(F32)
+    flow = (resid_v[...].astype(F32) + rms_norm(summed, gains[0].astype(F32))).astype(BF16).astype(F32)
     stream[...] = flow
-    in_send[...] = rms_norm(flow, gains[1:2]).astype(BF16)
+    in_send[...] = rms_norm(flow, gains[1].astype(F32)).astype(BF16)
 
     def in_slot(s):
         return inbuf.at[pl.ds(pl.multiple_of(s * SHARE, SHARE), SHARE)]
@@ -357,8 +483,19 @@
     def _():
         ag_copy(0).start()
 
-    for step in range(4, 9):
+    for step in range(6, 9):
         w_step(step)
+
+    ready("conv_value", "conv_gate")
+    last = conv_v.shape[2] - UP
+    for core in range(NC):
+        first = (x * NC + core) * NY * HID + y * HID
+        base = jnp.minimum(first // 128 * 128, last)
+        lanes = pl.ds(pl.multiple_of(base, 128), UP)
+        back = UP - (first - base)
+        v = pltpu.roll(conv_v[0, :, lanes].astype(F32), back, 1)
+        g = pltpu.roll(conv_v[1, :, lanes].astype(F32), back, 1)
+        taps[core, 0:3] = jnp.concatenate(side_lanes(v[:, :HID], g[:, :HID]), axis=1)
 
     @pl.loop(0, NZ)
     def _(k):
@@ -443,7 +580,7 @@
     for k in range(1, 16):
         projected += p_recv[k].astype(F32)
     projected = projected.astype(BF16).astype(F32)
-    out[...] = (stream[...] + rms_norm(projected, gains[2:3])).astype(BF16)
+    out[...] = (stream[...] + rms_norm(projected, gains[2].astype(F32))).astype(BF16)
 
     for copy in pending:
         copy.wait_send()
@@ -482,53 +619,14 @@
     conv_gate,
     down_weight,
 ):
-    tp = lax.axis_index(TP)
-    y = lax.axis_index("y")
-    sp = lax.axis_index(SP)
     scale = (query_nope.shape[2] + query_rope.shape[2]) ** (-0.5)
-    positions = sp * ROWS + jnp.arange(ROWS, dtype=jnp.int32)
-    key_positions = sp * ROWS + tp * SHARE + jnp.arange(SHARE, dtype=jnp.int32)
-
-    def own_rows(a):
-        return lax.dynamic_slice_in_dim(a, tp * SHARE, SHARE, 0)
-
-    normed = rms_norm(own_rows(latent).astype(F32), kv_gain.astype(F32)).astype(BF16)
-    key_turn = rotate(own_rows(rope_key).astype(F32), key_positions).astype(BF16)
-    query_turn = rotate(query_rope[:, 0].astype(F32), positions).astype(BF16)
-    kv_loc = jnp.concatenate([normed, key_turn, jnp.zeros((SHARE, 64), BF16)], axis=1)
-    q_loc = jnp.concatenate([query_nope[:, 0], query_turn, jnp.zeros((ROWS, 64), BF16)], axis=1)
-
-    width = up_value.shape[1] // NY
-    rest = width - 128
-
-    def by_y(a):
-        return jnp.transpose(a.reshape(a.shape[0], NY, width), (1, 0, 2))
-
-    def lanes(v, g):
-        pad = jnp.zeros(v.shape[:-1] + (64 - rest,), v.dtype)
-        return [v[..., :128], g[..., :128], v[..., 128:], pad, g[..., 128:], pad]
-
-    value, gate, down = by_y(up_value), by_y(up_gate), by_y(down_weight.T)
-    w_loc = jnp.concatenate(
-        lanes(value, gate) + [down, jnp.zeros(down.shape[:-1] + (256 - width,), BF16)], axis=-1
-    )
-
-    def chip_taps(core):
-        start = (tp // NC * NC + core) * width * NY + y * width
-        v = lax.dynamic_slice_in_dim(conv_value, start, width, 1)
-        g = lax.dynamic_slice_in_dim(conv_gate, start, width, 1)
-        return jnp.concatenate(lanes(v, g), axis=-1)
-
-    taps = jnp.stack([chip_taps(0), chip_taps(1)]).astype(F32)
-    taps = jnp.pad(taps, ((0, 0), (0, 5), (0, 0)))
-    gains = jnp.pad(jnp.stack([post_gain, pre_gain, ffn_gain]).astype(F32), ((0, 5), (0, 0)))
-
+    by_row, by_col = turn_tables()
     dma = pltpu.SemaphoreType.DMA
     vmem = pltpu.VMEM
     return pl.pallas_call(
         functools.partial(layer_kernel, scale),
         out_shape=jax.ShapeDtypeStruct((SHARE, D), BF16),
-        in_specs=[pl.BlockSpec(memory_space=vmem)] * 9,
+        in_specs=[pl.BlockSpec(memory_space=pl.ANY)] * 19,
         out_specs=pl.BlockSpec(memory_space=vmem),
         scratch_shapes=[
             vmem((KEYS, KW), BF16),
@@ -536,7 +634,7 @@
             vmem((NC, NZ * ROWS, WL), BF16),
             vmem((NC, 128, D), BF16),
             vmem((256, KEYS), BF16),
-            vmem((KEYS, 256), F32),
+            vmem((2, KEYS, 256), F32),
             vmem((4, 256, 256), F32),
             vmem((NT, 16, 128), F32),
             vmem((NT, 128, 128), BF16),
@@ -549,25 +647,56 @@
             vmem((TOK, D), BF16),
             vmem((NY * NX, SHARE, D), BF16),
             vmem((SHARE, D), F32),
+            vmem((SHARE, 256), BF16),
+            vmem((SHARE, 64), BF16),
+            vmem((1, 256), BF16),
+            vmem((ROWS, 128), BF16),
+            vmem((ROWS, 64), BF16),
+            vmem((8, 128), F32),
+            vmem((2, GRID, 128), F32),
+            vmem(up_value.shape, BF16),
+            vmem(up_gate.shape, BF16),
+            vmem(down_weight.shape, BF16),
+            vmem((256 * NT, 128), BF16),
+            vmem((256 * NT, 128), BF16),
+            vmem((SHARE, D), BF16),
+            vmem((3, 1, D), BF16),
+            vmem((2,) + conv_value.shape, BF16),
+            vmem((2, ROWS, 128), F32),
+            vmem((NY, 32, WL), BF16),
+            vmem((256 * NT, 128), F32),
+            vmem((4, 256, KW), BF16),
+            vmem((NT, 256, 128), BF16),
+            vmem((NC, 8, UP), F32),
         ]
         + [
             dma((n,))
-            for n in (15, 48, 64, 7, 8, 3, 4, 16, 16, 16, 16, 1, 1, 7, 8, 7, 8, 3, 4, 16, 16, 2, 2, 16, 16)
+            for n in (19, 15, 48, 64, 7, 8, 3, 4, 16, 16, 16, 16, 1, 1, 7, 8, 7, 8, 3, 4, 16, 16, 2, 2, 16, 16)
         ],
         compiler_params=pltpu.CompilerParams(
             collective_id=0, has_side_effects=True, vmem_limit_bytes=60 * 1024 * 1024
         ),
         name="layer",
     )(
-        kv_loc,
-        q_loc,
-        w_loc,
+        latent,
+        rope_key,
+        kv_gain[None],
+        query_nope[:, 0],
+        query_rope[:, 0],
+        by_row,
+        by_col,
+        up_value,
+        up_gate,
+        down_weight,
         out_weight,
-        key_up.reshape(key_up.shape[0], -1),
-        value_up.reshape(value_up.shape[0], -1),
-        own_rows(residual),
-        gains,
-        taps,
+        key_up.reshape(-1, key_up.shape[2]),
+        value_up.reshape(-1, value_up.shape[2]),
+        residual,
+        post_gain[None],
+        pre_gain[None],
+        ffn_gain[None],
+        conv_value,
+        conv_gate,
     )
 
 

time: 122 us -> 104 us (0.85)
  Pallas kernels: 107 us -> 96.7 us
  other arithmetic: 4.52 us -> 0 us
  local copies, waits for them, and re-layouts: 10 us -> 6.88 us
    pallas_call x1, Pallas kernels: 107 us -> 96.7 us  [body(): pl.pallas_call(functools.partial(layer_kernel, scale), out_shape=jax.Shap...]
    broadcast_in_dim x3 -> x4, local copies, waits for them, and re-layouts: 0.02 us -> 2.39 us  [the longest x1 0.61 us: body(): ffn_gain[None]]
    slice x7 -> x0, local copies, waits for them, and re-layouts: 1.65 us -> none  [the longest x6 1.64 us: lanes(): return [v[..., :128], g[..., :128], v[..., 128:], pad, g[..., 128:], pad]]
    reshape x7 -> x0, local copies, waits for them, and re-layouts: 1.52 us -> none  [the longest x1 1.19 us: body(): value_up.reshape(value_up.shape[0], -1)]
    pad x2 -> x0, other arithmetic: 1.28 us -> none  [the longest x1 0.66 us: body(): jnp.pad(jnp.stack([post_gain, pre_gain, ffn_gain]).astype(F32), ((0, 5),...]
    concatenate x2 -> x0, other arithmetic: 1.25 us -> none  [the longest x1 0.65 us: body(): jnp.concatenate([query_nope[:, 0], query_turn, jnp.zeros((ROWS, 64), BF16...]
    unnamed x29 -> x18, local copies, waits for them, and re-layouts: 4.68 us -> 4.49 us
where the time goes in v2:
time: 104 us
  Pallas kernels  96.7 us (93%)
  local copies, waits for them, and re-layouts  6.88 us (7%)
    pallas_call x1, Pallas kernels, body(): pl.pallas_call(functools.partial(layer_kernel, scale), out_shape=jax.Shap...  96.7 us
    unnamed x18, local copies, waits for them, and re-layouts  4.49 us

profile of v2, /device:TPU:1, one launch (start us, length us, event | category | flops | bytes accessed | tf_op | source)
XLA Modules:
  0.0 103.6 jit_solution(6875886655997444275)
XLA Ops:
  0.0 0.0 copy-start.3
  0.0 0.0 copy-start.6
  0.0 0.7 copy-done.6
  0.7 0.0 copy-start.4
  0.7 0.6 broadcast_in_dim.12.kv_gain
  1.3 0.0 copy-done.3
  1.3 0.0 copy-start.1
  1.3 0.6 broadcast_in_dim.13.post_gain
  1.9 0.0 copy-done.4
  1.9 0.0 copy-start.5
  1.9 0.6 broadcast_in_dim.14.pre_gain
  2.5 0.1 copy-done.5
  2.6 0.0 copy-start.2
  2.6 0.6 broadcast_in_dim.15.ffn_gain
  3.2 0.0 copy-done.1
  3.2 0.0 copy-start
  3.2 0.7 copy.20
  3.9 0.0 copy-done.2
  3.9 0.7 copy.21.rope_key
  4.6 0.0 copy-done
  4.6 0.8 copy.22.down
  5.4 96.7 %layer.1 = bf16[16,2048]{1,0:T(8,128)(2,1)} custom-call(bf16[128,256]{1,0:T(8,128)(2,1)} %latent.1, bf16[128,64]{1,0:T(8,128)(2,1)} %copy.21.rope_key, bf16[1,256]{1,0:T(2,128)(2,1)} %broadcast_in_dim.12.kv_gain, bf16[128,128]{1,0:T(8,128)(2,1)} %bitcast.7, bf16[128,64]{1,0:T(8,128)(2,1)} %bitcast.6, f32[64,8,128]{2,1,0:T(8,128)} %constant.4.clone.by_row, ...), custom_call_target="tpu_custom_call" | custom-call | tf_op jit(solution)/shard_map/layer/pallas_call | solution.py:626
  102.1 1.5 %copy.24 = bf16[16,2048]{1,0:T(8,128)(2,1)} copy(bf16[16,2048]{1,0:T(8,128)(2,1)} %layer.1) | data formatting | bytes 131072
Async XLA Ops:
  0.0 1.3 %copy-start.3 = (bf16[2048]{0:T(1024)(128)(2,1)S(1)}, bf16[2048]{0:T(1024)(128)(2,1)}, u32[]{:S(2)}) copy-start(bf16[2048]{0:T(1024)(128)(2,1)} %param.28) | copy-start | bytes 12292
  0.0 0.7 copy-start.6
  0.7 1.2 %copy-start.4 = (bf16[2048]{0:T(1024)(128)(2,1)S(1)}, bf16[2048]{0:T(1024)(128)(2,1)}, u32[]{:S(2)}) copy-start(bf16[2048]{0:T(1024)(128)(2,1)} %param.29) | copy-start | bytes 12292
  1.3 1.9 %copy-start.1 = (bf16[128,1,64]{0,2,1:T(8,128)(2,1)S(1)}, bf16[128,1,64]{0,2,1:T(8,128)(2,1)}, u32[]{:S(2)}) copy-start(bf16[128,1,64]{0,2,1:T(8,128)(2,1)} %param.21) | copy-start | bytes 49156
  1.9 0.7 copy-start.5
  2.6 1.3 %copy-start.2 = (bf16[128,64]{0,1:T(8,128)(2,1)S(1)}, bf16[128,64]{0,1:T(8,128)(2,1)}, u32[]{:S(2)}) copy-start(bf16[128,64]{0,1:T(8,128)(2,1)} %param.23) | copy-start | bytes 49156
  3.2 1.4 %copy-start = (bf16[704,32]{0,1:T(8,128)(2,1)S(1)}, bf16[704,32]{0,1:T(8,128)(2,1)}, u32[]{:S(2)}) copy-start(bf16[704,32]{0,1:T(8,128)(2,1)} %param.35) | copy-start | bytes 135172

commit v3 on v2

--- a/solution.py
+++ b/solution.py
@@ -29,10 +29,12 @@
 KEYS = NZ * NY * SHARE
 QW = 256
 KW = 384
-WL = 640
 UP = 384
 HID = 176
-W_AT = {1: 0, 5: 1, 8: 2}
+W_AT = {2: [0], 6: [1], 8: [2]}
+W_KVY = {1: [3], 2: [4]}
+W_ATTN = {1: [5], 3: [6]}
+W_MORE = ([7, 8], [9, 10], [11, 12, 13, 14, 15, 16])
 TOK = 256
 
 
@@ -66,8 +68,14 @@
     return values * cosine + other * sine
 
 
-def widen64(values):
-    return jnp.concatenate([values.astype(F32), jnp.zeros(values.shape, F32)], axis=1)
+def in_one_row(ref):
+    folded = ref[...].astype(F32)
+    return jnp.concatenate([folded[i : i + 1] for i in range(folded.shape[0])], axis=1)
+
+
+def as_rows(columns):
+    both = jnp.concatenate([columns.astype(F32), jnp.zeros(columns.shape, F32)], axis=0)
+    return both.T
 
 
 def dot_nn(a, b):
@@ -88,7 +96,6 @@
     scale,
     latent,
     rope_key,
-    kv_gain,
     q_nope,
     q_rope,
     by_row,
@@ -100,6 +107,7 @@
     key_up,
     value_up,
     resid,
+    kv_gain,
     post_gain,
     pre_gain,
     ffn_gain,
@@ -109,10 +117,12 @@
     kvbuf,
     qbuf,
     wbuf,
+    dbuf,
+    d_stage,
     owbuf,
     kvt,
     s_scr,
-    ot_scr,
+    st_send,
     stats,
     o_send,
     o_recv,
@@ -126,7 +136,6 @@
     stream,
     latent_v,
     rope_key_v,
-    kv_gain_v,
     q_nope_v,
     q_rope_v,
     by_row_v,
@@ -137,10 +146,13 @@
     key_up_v,
     value_up_v,
     resid_v,
+    kv_gain_v,
     gains,
     conv_v,
     turns,
+    key_rows,
     w_loc,
+    d_loc,
     wide,
     qf,
     vu,
@@ -208,10 +220,13 @@
         local[name].start()
 
     load("latent", own(latent), latent_v)
-    load("rope_key", own(rope_key), rope_key_v)
+    load("rope_key", rope_key, rope_key_v)
     load("by_row", by_row.at[z * NY + y], by_row_v)
     load("by_col", by_col, by_col_v)
     load("kv_gain", kv_gain, kv_gain_v)
+    load("post", post_gain, gains.at[0])
+    load("pre", pre_gain, gains.at[1])
+    load("ffn", ffn_gain, gains.at[2])
     load("q_nope", q_nope, q_nope_v)
     load("q_rope", q_rope, q_rope_v)
     load("up_value", up_value, up_value_v)
@@ -221,9 +236,6 @@
     load("key_up", key_up, key_up_v)
     load("value_up", value_up, value_up_v)
     load("resid", own(resid), resid_v)
-    load("post", post_gain, gains.at[0])
-    load("pre", pre_gain, gains.at[1])
-    load("ffn", ffn_gain, gains.at[2])
     load("conv_value", conv_value, conv_v.at[0])
     load("conv_gate", conv_gate, conv_v.at[1])
 
@@ -243,11 +255,16 @@
         start = pl.multiple_of((yy * NZ + k) * SHARE, SHARE)
         return kvbuf.at[pl.ds(start, SHARE)]
 
-    def w_slot(core, k):
-        return wbuf.at[core, pl.ds(pl.multiple_of(k * ROWS, ROWS), ROWS)]
-
-    def w_part(k, yy):
-        return wbuf.at[c, pl.ds(pl.multiple_of(k * ROWS + yy * 32, 32), 32)]
+    def w_slot(kind, core, k):
+        at = pl.ds(pl.multiple_of(k * ROWS, ROWS), ROWS)
+        if kind == 0:
+            return wbuf.at[core, at]
+        return dbuf.at[core, pl.ds(0, HID), at]
+
+    def w_part(kind, yy):
+        if kind == 0:
+            return wbuf.at[c, pl.ds(pl.multiple_of(z * ROWS + yy * 32, 32), 32)]
+        return d_stage.at[pl.ds(pl.multiple_of(yy * 32, 32), 32)]
 
     ready("latent", "rope_key", "by_row", "by_col", "kv_gain")
     for i in range(2):
@@ -257,11 +274,10 @@
         turns[i] = jnp.concatenate(grid_rows, axis=0)
     rows = pl.ds(pl.multiple_of(tp * SHARE, SHARE), SHARE)
     kv_slot(y, z)[:, :256] = rms_norm(
-        latent_v[...].astype(F32), kv_gain_v[...].astype(F32)
+        latent_v[...].astype(F32), in_one_row(kv_gain_v)
     ).astype(BF16)
-    kv_slot(y, z)[:, 256:] = turned(
-        widen64(rope_key_v[...]), turns[0, rows], turns[1, rows]
-    ).astype(BF16)
+    key_rows[...] = as_rows(rope_key_v[...])
+    kv_slot(y, z)[:, 256:] = turned(key_rows[rows], turns[0, rows], turns[1, rows]).astype(BF16)
 
     pl.semaphore_wait(barrier, 5 + PLANE - 1)
 
@@ -288,60 +304,74 @@
     kv_to_y(z, 0)
     ready("q_nope", "q_rope")
     qbuf[tp, :, :128] = q_nope_v[...]
-    qbuf[tp, :, 128:] = turned(widen64(q_rope_v[...]), turns[0], turns[1]).astype(BF16)
+    qbuf[tp, :, 128:] = turned(as_rows(q_rope_v[...]), turns[0], turns[1]).astype(BF16)
     for j in range(1, NT):
         t = (tp + j) % NT
         go(push(qbuf.at[tp], qbuf.at[tp], qs.at[j - 1], qr.at[tp], tp_peer(t)))
 
     ready("up_value", "up_gate", "down")
-    eye = (
-        lax.broadcasted_iota(jnp.int32, (32, 32), 0) == lax.broadcasted_iota(jnp.int32, (32, 32), 1)
-    ).astype(BF16)
     value, gate = up_value_v[...].astype(F32), up_gate_v[...].astype(F32)
-    across = dot_nt(eye, down_v[...])
+    across = down_v[...].astype(F32)
     for yy in range(NY):
         at = slice(yy * HID, (yy + 1) * HID)
         parts = side_lanes(value[:, at], gate[:, at])
-        parts += [across[:, at], jnp.zeros((32, 256 - HID), F32)]
         w_loc[yy] = jnp.concatenate(parts, axis=1).astype(BF16)
+        parts = [across[:, at], jnp.zeros((32, 256 - HID), F32)]
+        d_loc[yy] = jnp.concatenate(parts, axis=1).astype(BF16)
     for j in range(1, NY):
         yy = (y + j) % NY
-        go(push(w_loc.at[yy], w_part(z, y), wys.at[j - 1], wyr.at[y], (z, yy, x, c)))
-    w_part(z, y)[...] = w_loc[y]
+        dev = (z, yy, x, c)
+        go(push(w_loc.at[yy], w_part(0, y), wys.at[j - 1], wyr.at[y], dev))
+        go(push(d_loc.at[yy], w_part(1, y), wys.at[j + 2], wyr.at[NY + y], dev))
+    w_part(0, y)[...] = w_loc[y]
+    w_part(1, y)[...] = d_loc[y]
+    dbuf[:, HID:] = jnp.zeros((NC, 256 - HID, D), BF16)
     ready("ow")
     go(push(owbuf.at[c], owbuf.at[c], ows.at[0], owr.at[0], partner))
 
-    def w_send(k, step, to_right, to_left):
-        slot = w_slot(c, k)
+    def w_send(kind, k, step, to_right, to_left):
+        slot = w_slot(kind, c, k)
         if to_right:
-            go(push(slot, slot, wzs.at[step], wzr.at[k], right))
+            go(push(slot, slot, wzs.at[kind, step], wzr.at[kind, k], right))
         if to_left:
-            go(push(slot, slot, wzs.at[8 + step], wzr.at[k], left))
-
-    def w_across(k, sem):
-        slot = w_slot(c, k)
-        go(push(slot, slot, wps.at[sem], wpr.at[k], partner))
-
-    def w_step(step):
-        if step == 0:
+            go(push(slot, slot, wzs.at[kind, 8 + step], wzr.at[kind, k], left))
+
+    def w_across(kind, k, sem):
+        slot = w_slot(kind, c, k)
+        go(push(slot, slot, wps.at[kind, sem], wpr.at[kind, k], partner))
+
+    def w_wait(kind, k, dev):
+        slot = w_slot(kind, c, k)
+        push(slot, slot, wzs.at[kind, 0], wzr.at[kind, k], dev).wait_recv()
+
+    def w_start():
+        for kind in range(2):
             for j in range(1, NY):
                 yy = (y + j) % NY
-                part = w_part(z, yy)
-                push(part, part, wys.at[j - 1], wyr.at[yy], (z, yy, x, c)).wait_recv()
-            w_send(z, 0, True, True)
-            w_across(z, 0)
-            return
-        k = zz(-step)
-        slot = w_slot(c, k)
-        push(slot, slot, wzs.at[0], wzr.at[k], left).wait_recv()
-        w_send(k, step, step < 8, False)
-        w_across(k, 2 * step - 1)
-        if step < 8:
-            k = zz(step)
-            slot = w_slot(c, k)
-            push(slot, slot, wzs.at[0], wzr.at[k], right).wait_recv()
-            w_send(k, step, False, step < 7)
-            w_across(k, 2 * step)
+                part = w_part(kind, yy)
+                sem = wyr.at[kind * NY + yy]
+                push(part, part, wys.at[0], sem, (z, yy, x, c)).wait_recv()
+            if kind == 1:
+                columns = pl.ds(pl.multiple_of(z * ROWS, ROWS), ROWS)
+                dbuf[c, :HID, columns] = d_stage[...].astype(F32).T[:HID].astype(BF16)
+            w_send(kind, z, 0, True, True)
+            w_across(kind, z, 0)
+
+    def w_go(steps):
+        for event in steps:
+            if event == 0:
+                w_start()
+                continue
+            step, kind = (event + 1) // 2, (event + 1) % 2
+            k = zz(-step)
+            w_wait(kind, k, left)
+            w_send(kind, k, step, step < 8, False)
+            w_across(kind, k, 2 * step - 1)
+            if step < 8:
+                k = zz(step)
+                w_wait(kind, k, right)
+                w_send(kind, k, step, False, step < 7)
+                w_across(kind, k, 2 * step)
 
     def kv_wait(yy, k):
         slot = kv_slot(yy, k)
@@ -355,15 +385,19 @@
         wide[...] = key_up_v[...].astype(F32)
         for h in range(NT):
             up_h = wide[pl.ds(h, 256, stride=NT)].astype(BF16)
-            r = slice(h % 2 * 128, h % 2 * 128 + 128)
-            qf[h // 2, r, :256] = dot_nt(qbuf[h, :, :128], up_h).astype(BF16)
-            qf[h // 2, r, 256:] = qbuf[h, :, 128:]
+            folded = dot_nt(qbuf[h, :, :128], up_h).astype(BF16)
+            folded = folded.reshape(NX, NC, SHARE, 256)
+            rope = qbuf[h, :, 128:].reshape(NX, NC, SHARE, 128)
+            for core in range(NC):
+                r = slice(core * 128 + h % 2 * 64, core * 128 + h % 2 * 64 + 64)
+                qf[h // 2, r, :256] = folded[:, core].reshape(64, 256)
+                qf[h // 2, r, 256:] = rope[:, core].reshape(64, 128)
 
     def split_values():
         ready("value_up")
         wide[...] = value_up_v[...].astype(F32)
         for h in range(NT):
-            vu[h] = wide[pl.ds(h, 256, stride=NT)].astype(BF16)
+            vu[h // 2, h % 2 * 128 : h % 2 * 128 + 128] = wide[pl.ds(h, 256, stride=NT)].T.astype(BF16)
 
     for d in range(1, 9):
         if d == 4:
@@ -383,7 +417,7 @@
         if d < 8:
             kv_to_y(k2, 2 * d)
         if d in W_AT:
-            w_step(W_AT[d])
+            w_go(W_AT[d])
     for j in range(1, NY):
         yy = (y + j) % NY
 
@@ -391,56 +425,57 @@
         def _(k):
             kv_wait(yy, k)
 
+        if j in W_KVY:
+            w_go(W_KVY[j])
+
     kvt[...] = kvbuf[:, :256].T
-    for hp in range(4):
-        s_now = s_scr.at[hp % 2]
+    lane = lax.broadcasted_iota(jnp.int32, (128, 256), 1)
+    for i in range(NX):
+        hp = (x + 1 + i) % NX
+        s_now = s_scr.at[i % 2]
         s_now[...] = dot_nt(kvbuf[...], qf[hp])
         top = jnp.max(s_now[...], axis=0, keepdims=True)
         weights = jnp.exp((s_now[...] - top) * scale)
         total = jnp.sum(weights, axis=0, keepdims=True)
-        ot_scr[hp] = dot_nn(kvt[...], weights.astype(BF16))
-        for i in range(2):
-            h = 2 * hp + i
-            stats[tp, h : h + 1] = top[:, i * 128 : (i + 1) * 128]
-            stats[tp, 8 + h : 9 + h] = total[:, i * 128 : (i + 1) * 128]
-        if hp == 1:
-            w_step(3)
-
-    for j in range(1, NT):
-        t = (tp + j) % NT
-        go(push(stats.at[tp], stats.at[tp], sts.at[j - 1], str_.at[tp], tp_peer(t)))
-    w_step(4)
+        mixed = dot_nn(kvt[...], weights.astype(BF16))
+        mixed = dot_nn(vu[hp], mixed.astype(BF16))
+        mixed = jnp.where((lane & 64) == 0, mixed[:128], mixed[128:]).astype(BF16)
+        for core in range(NC):
+            t = hp * NC + core
+            at = slice(core * 128, core * 128 + 128)
+            o_send[t] = mixed[:, at]
+            st_send[t, 0:1] = top[:, at]
+            st_send[t, 1:2] = total[:, at]
+        if i < NX - 1:
+            for core in range(NC):
+                t = hp * NC + core
+                j = i * NC + core
+                go(push(st_send.at[t], stats.at[tp], sts.at[j], str_.at[tp], tp_peer(t)))
+                go(push(o_send.at[t], o_recv.at[tp], os_.at[j], or_.at[tp], tp_peer(t)))
+        else:
+            t = x * NC + 1 - c
+            go(push(st_send.at[t], stats.at[tp], sts.at[6], str_.at[tp], partner))
+            go(push(o_send.at[t], o_recv.at[tp], os_.at[6], or_.at[tp], partner))
+            o_recv[tp] = o_send[tp]
+            stats[tp] = st_send[tp]
+        if i in W_ATTN:
+            w_go(W_ATTN[i])
+    w_go(W_MORE[0])
+    push(owbuf.at[1 - c], owbuf.at[1 - c], ows.at[0], owr.at[0], partner).wait_recv()
     for j in range(1, NT):
         t = (tp + j) % NT
         push(stats.at[t], stats.at[t], sts.at[0], str_.at[t], tp_peer(t)).wait_recv()
-    top_all = stats[0, 0:8]
+        push(o_recv.at[t], o_recv.at[t], os_.at[0], or_.at[t], tp_peer(t)).wait_recv()
+    top_all = stats[0, 0:1]
     for t in range(1, NT):
-        top_all = jnp.maximum(top_all, stats[t, 0:8])
+        top_all = jnp.maximum(top_all, stats[t, 0:1])
     total_all = jnp.zeros_like(top_all)
+    attended = jnp.zeros((128, 128), F32)
     for t in range(NT):
-        total_all += jnp.exp((stats[t, 0:8] - top_all) * scale) * stats[t, 8:16]
-    factor = jnp.exp((stats[tp, 0:8] - top_all) * scale) / total_all
-    for hp in range(4):
-        for i in range(2):
-            h = 2 * hp + i
-            scaled = ot_scr[hp, :, i * 128 : (i + 1) * 128] * factor[h : h + 1]
-            mixed = dot_nn(scaled.T.astype(BF16), vu[h])
-            blocks = mixed.astype(BF16).reshape(NX, NC, SHARE, 128)
-            for core in range(NC):
-                o_send[hp * NC + core, i * 64 : (i + 1) * 64] = blocks[:, core].reshape(64, 128)
-    for j in range(1, NT):
-        t = (tp + j) % NT
-        go(push(o_send.at[t], o_recv.at[tp], os_.at[j - 1], or_.at[tp], tp_peer(t)))
-    o_recv[tp] = o_send[tp]
-    w_step(5)
-    push(owbuf.at[1 - c], owbuf.at[1 - c], ows.at[0], owr.at[0], partner).wait_recv()
-    for j in range(1, NT):
-        t = (tp + j) % NT
-        push(o_recv.at[t], o_recv.at[t], os_.at[0], or_.at[t], tp_peer(t)).wait_recv()
-    attended = o_recv[0].astype(F32)
-    for t in range(1, NT):
-        attended += o_recv[t].astype(F32)
-    attended = attended.astype(BF16)
+        factor = jnp.exp((stats[t, 0:1] - top_all) * scale)
+        total_all += factor * stats[t, 1:2]
+        attended += factor * o_recv[t].astype(F32)
+    attended = (attended / total_all).T.astype(BF16)
     r_send[...] = (
         dot_nn(attended[:64], owbuf[0]) + dot_nn(attended[64:], owbuf[1])
     ).astype(BF16)
@@ -449,6 +484,7 @@
         src = r_send.at[pl.ds(pl.multiple_of(xx * SHARE, SHARE), SHARE)]
         go(push(src, r_recv.at[x], rss.at[j - 1], rsr.at[x], (z, y, xx, c)))
     r_recv[x] = r_send[pl.ds(pl.multiple_of(x * SHARE, SHARE), SHARE)]
+    w_go(W_MORE[1])
     for j in range(1, NX):
         xx = (x + j) % NX
         push(r_recv.at[xx], r_recv.at[xx], rss.at[0], rsr.at[xx], (z, y, xx, c)).wait_recv()
@@ -457,9 +493,9 @@
     for j in range(1, NX):
         summed += r_recv[j].astype(F32)
     summed = summed.astype(BF16).astype(F32)
-    flow = (resid_v[...].astype(F32) + rms_norm(summed, gains[0].astype(F32))).astype(BF16).astype(F32)
+    flow = (resid_v[...].astype(F32) + rms_norm(summed, in_one_row(gains.at[0]))).astype(BF16).astype(F32)
     stream[...] = flow
-    in_send[...] = rms_norm(flow, gains[1].astype(F32)).astype(BF16)
+    in_send[...] = rms_norm(flow, in_one_row(gains.at[1])).astype(BF16)
 
     def in_slot(s):
         return inbuf.at[pl.ds(pl.multiple_of(s * SHARE, SHARE), SHARE)]
@@ -483,8 +519,7 @@
     def _():
         ag_copy(0).start()
 
-    for step in range(6, 9):
-        w_step(step)
+    w_go(W_MORE[2])
 
     ready("conv_value", "conv_gate")
     last = conv_v.shape[2] - UP
@@ -499,8 +534,8 @@
 
     @pl.loop(0, NZ)
     def _(k):
-        slot = w_slot(1 - c, k)
-        push(slot, slot, wps.at[0], wpr.at[k], partner).wait_recv()
+        slot = w_slot(0, 1 - c, k)
+        push(slot, slot, wps.at[0, 0], wpr.at[0, k], partner).wait_recv()
 
     own_slot = jnp.where(half == c, mine, -1)
 
@@ -511,12 +546,54 @@
             push(in_slot(s), in_slot(s), ags.at[0], agr.at[s], partner).wait_recv()
 
     for core in range(NC):
-        up[core, 8 : 8 + TOK] = dot_nn(inbuf[...], wbuf[core, :, :UP])
+        up[core, 8 : 8 + TOK] = dot_nn(inbuf[...], wbuf[core])
 
     low_dev = ((z + c) % NZ, y, x, 1 - c)
     high_dev = ((z + c - 1 + NZ) % NZ, y, x, 1 - c)
     go(push(up.at[:, pl.ds(TOK, 8)], up.at[:, pl.ds(0, 8)], hs.at[0], hr.at[0], low_dev))
     go(push(up.at[:, pl.ds(8, 8)], up.at[:, pl.ds(TOK + 8, 8)], hs.at[1], hr.at[1], high_dev))
+    def hidden_rows(core, first, count):
+        conv = (
+            up[core, first + 7 : first + 7 + count] * taps[core, 0:1]
+            + up[core, first + 8 : first + 8 + count] * taps[core, 1:2]
+            + up[core, first + 9 : first + 9 + count] * taps[core, 2:3]
+        )
+        gate = conv[:, 128:256]
+        near = gate / (1.0 + jnp.exp(-gate)) * conv[:, :128]
+        gate = pltpu.roll(conv[:, 256:], 64, 1)
+        far = gate / (1.0 + jnp.exp(-gate)) * conv[:, 256:]
+        lane = lax.broadcasted_iota(jnp.int32, far.shape, 1)
+        far = jnp.where(lane < 64, far, 0.0)
+        return jnp.concatenate([near.astype(BF16), far.astype(BF16)], axis=1)
+
+    def down_rows(hidden):
+        return (dot_nn(hidden[0], dbuf[0]) + dot_nn(hidden[1], dbuf[1])).astype(BF16)
+
+    inner = [hidden_rows(core, SHARE, TOK - 2 * SHARE) for core in range(NC)]
+    @pl.loop(0, NZ)
+    def _(k):
+        slot = w_slot(1, 1 - c, k)
+        push(slot, slot, wps.at[1, 0], wpr.at[1, k], partner).wait_recv()
+
+    p_send[SHARE : TOK - SHARE] = down_rows(inner)
+
+    chip = y * NX + x
+
+    def p_slot(s):
+        return p_send.at[pl.ds(pl.multiple_of(s * SHARE, SHARE), SHARE)]
+
+    def rs_copy(s):
+        dev = (z, 2 * c + s // NT, (s // NC) % NX, s % NC)
+        return push(p_slot(s), p_recv.at[chip], ps.at[s], pr.at[chip], dev)
+
+    @pl.loop(0, 16)
+    def _(j):
+        s = (mine + j) % 16
+
+        @pl.when((s != own_slot) & (s > 0) & (s < 15))
+        def _():
+            rs_copy(s).start()
+
     low, high = up.at[:, pl.ds(0, 8)], up.at[:, pl.ds(TOK + 8, 8)]
     push(low, low, hs.at[0], hr.at[0], low_dev).wait_recv()
     push(high, high, hs.at[1], hr.at[1], high_dev).wait_recv()
@@ -529,40 +606,21 @@
     def _():
         up[:, TOK + 8 : TOK + 16] = jnp.zeros((NC, 8, UP), F32)
 
-    hidden = []
-    for core in range(NC):
-        conv = (
-            up[core, 7 : 7 + TOK] * taps[core, 0:1]
-            + up[core, 8 : 8 + TOK] * taps[core, 1:2]
-            + up[core, 9 : 9 + TOK] * taps[core, 2:3]
+    outer = [
+        jnp.concatenate(
+            [hidden_rows(core, 0, SHARE), hidden_rows(core, TOK - SHARE, SHARE)], axis=0
         )
-        gate = conv[:, 128:256]
-        first = gate / (1.0 + jnp.exp(-gate)) * conv[:, :128]
-        gate = pltpu.roll(conv[:, 256:], 64, 1)
-        second = gate / (1.0 + jnp.exp(-gate)) * conv[:, 256:]
-        lane = lax.broadcasted_iota(jnp.int32, second.shape, 1)
-        second = jnp.where(lane < 64, second, 0.0)
-        hidden.append(jnp.concatenate([first.astype(BF16), second.astype(BF16)], axis=1))
-    p_send[...] = (
-        dot_nt(hidden[0], wbuf[0, :, UP:]) + dot_nt(hidden[1], wbuf[1, :, UP:])
-    ).astype(BF16)
-
-    chip = y * NX + x
-
-    def p_slot(s):
-        return p_send.at[pl.ds(pl.multiple_of(s * SHARE, SHARE), SHARE)]
-
-    def rs_copy(s):
-        dev = (z, 2 * c + s // NT, (s // NC) % NX, s % NC)
-        return push(p_slot(s), p_recv.at[chip], ps.at[s], pr.at[chip], dev)
-
-    @pl.loop(0, 16)
-    def _(j):
-        s = (mine + j) % 16
+        for core in range(NC)
+    ]
+    edges = down_rows(outer)
+    p_send[:SHARE] = edges[:SHARE]
+    p_send[TOK - SHARE :] = edges[SHARE:]
+    for s in (0, 15):
 
         @pl.when(s != own_slot)
         def _():
             rs_copy(s).start()
+
 
     @pl.when(half == c)
     def _():
@@ -580,7 +638,7 @@
     for k in range(1, 16):
         projected += p_recv[k].astype(F32)
     projected = projected.astype(BF16).astype(F32)
-    out[...] = (stream[...] + rms_norm(projected, gains[2].astype(F32))).astype(BF16)
+    out[...] = (stream[...] + rms_norm(projected, in_one_row(gains.at[2]))).astype(BF16)
 
     for copy in pending:
         copy.wait_send()
@@ -621,6 +679,7 @@
 ):
     scale = (query_nope.shape[2] + query_rope.shape[2]) ** (-0.5)
     by_row, by_col = turn_tables()
+
     dma = pltpu.SemaphoreType.DMA
     vmem = pltpu.VMEM
     return pl.pallas_call(
@@ -631,12 +690,14 @@
         scratch_shapes=[
             vmem((KEYS, KW), BF16),
             vmem((NT, ROWS, QW), BF16),
-            vmem((NC, NZ * ROWS, WL), BF16),
+            vmem((NC, NZ * ROWS, UP), BF16),
+            vmem((NC, 256, D), BF16),
+            vmem((ROWS, 256), BF16),
             vmem((NC, 128, D), BF16),
             vmem((256, KEYS), BF16),
             vmem((2, KEYS, 256), F32),
-            vmem((4, 256, 256), F32),
-            vmem((NT, 16, 128), F32),
+            vmem((NT, 8, 128), F32),
+            vmem((NT, 8, 128), F32),
             vmem((NT, 128, 128), BF16),
             vmem((NT, 128, 128), BF16),
             vmem((64, D), BF16),
@@ -648,30 +709,34 @@
             vmem((NY * NX, SHARE, D), BF16),
             vmem((SHARE, D), F32),
             vmem((SHARE, 256), BF16),
-            vmem((SHARE, 64), BF16),
-            vmem((1, 256), BF16),
+            vmem((64, ROWS), BF16),
             vmem((ROWS, 128), BF16),
-            vmem((ROWS, 64), BF16),
+            vmem((64, ROWS), BF16),
             vmem((8, 128), F32),
             vmem((2, GRID, 128), F32),
             vmem(up_value.shape, BF16),
             vmem(up_gate.shape, BF16),
-            vmem(down_weight.shape, BF16),
+            vmem(down_weight.shape[::-1], BF16),
             vmem((256 * NT, 128), BF16),
             vmem((256 * NT, 128), BF16),
             vmem((SHARE, D), BF16),
-            vmem((3, 1, D), BF16),
+            vmem((2, 128), BF16),
+            vmem((3, D // 128, 128), BF16),
             vmem((2,) + conv_value.shape, BF16),
             vmem((2, ROWS, 128), F32),
-            vmem((NY, 32, WL), BF16),
+            vmem((ROWS, 128), F32),
+            vmem((NY, 32, UP), BF16),
+            vmem((NY, 32, 256), BF16),
             vmem((256 * NT, 128), F32),
             vmem((4, 256, KW), BF16),
-            vmem((NT, 256, 128), BF16),
+            vmem((4, 256, 256), BF16),
             vmem((NC, 8, UP), F32),
         ]
+        + [dma((n,)) for n in (19, 15, 48, 64, 7, 8, 6, 8)]
+        + [dma((2, 16))] * 4
         + [
             dma((n,))
-            for n in (19, 15, 48, 64, 7, 8, 3, 4, 16, 16, 16, 16, 1, 1, 7, 8, 7, 8, 3, 4, 16, 16, 2, 2, 16, 16)
+            for n in (1, 1, 7, 8, 7, 8, 3, 4, 16, 16, 2, 2, 16, 16)
         ],
         compiler_params=pltpu.CompilerParams(
             collective_id=0, has_side_effects=True, vmem_limit_bytes=60 * 1024 * 1024
@@ -679,22 +744,22 @@
         name="layer",
     )(
         latent,
-        rope_key,
-        kv_gain[None],
+        rope_key.T,
         query_nope[:, 0],
-        query_rope[:, 0],
+        query_rope[:, 0].T,
         by_row,
         by_col,
         up_value,
         up_gate,
-        down_weight,
+        down_weight.T,
         out_weight,
         key_up.reshape(-1, key_up.shape[2]),
         value_up.reshape(-1, value_up.shape[2]),
         residual,
-        post_gain[None],
-        pre_gain[None],
-        ffn_gain[None],
+        kv_gain.reshape(-1, 128),
+        post_gain.reshape(-1, 128),
+        pre_gain.reshape(-1, 128),
+        ffn_gain.reshape(-1, 128),
         conv_value,
         conv_gate,
     )

time: 104 us -> 85.1 us (0.82)
  Pallas kernels: 96.7 us -> 82.7 us
  local copies, waits for them, and re-layouts: 6.88 us -> 1.47 us
    pallas_call x1, Pallas kernels: 96.7 us -> 82.7 us  [body(): pl.pallas_call(functools.partial(layer_kernel, scale), out_shape=jax.Shap...]
    unnamed x18 -> x1, local copies, waits for them, and re-layouts: 4.49 us -> 1.47 us
    broadcast_in_dim x4 -> x0, local copies, waits for them, and re-layouts: 2.39 us -> none  [the longest x1 0.61 us: body(): ffn_gain[None]]
where the time goes in v3:
time: 85.1 us; the launch traced here: 84.2 us
  Pallas kernels  82.7 us (97%)
  local copies, waits for them, and re-layouts  1.47 us (2%)
    pallas_call x1, Pallas kernels, body(): pl.pallas_call(functools.partial(layer_kernel, scale), out_shape=jax.Shap...  82.7 us

profile of v3, /device:TPU:1, one launch (start us, length us, event | category | flops | bytes accessed | tf_op | source)
XLA Modules:
  0.0 84.2 jit_solution(17163010334744219931)
XLA Ops:
  0.0 82.7 %layer.1 = bf16[16,2048]{1,0:T(8,128)(2,1)} custom-call(bf16[128,256]{1,0:T(8,128)(2,1)} %latent.1, bf16[64,128]{1,0:T(8,128)(2,1)} %bitcast.16, bf16[128,128]{1,0:T(8,128)(2,1)} %bitcast.15, bf16[64,128]{1,0:T(8,128)(2,1)} %bitcast.17, f32[64,8,128]{2,1,0:T(8,128)} %constant.4.clone.by_row, f32[2,64,128]{2,1,0:T(8,128)} %constant.5.clone.by_col, ...), custom_call_target="tpu_custom_call" | custom-call | tf_op jit(solution)/shard_map/layer/pallas_call | solution.py:685
  82.7 1.5 %copy.21 = bf16[16,2048]{1,0:T(8,128)(2,1)} copy(bf16[16,2048]{1,0:T(8,128)(2,1)} %layer.1) | data formatting | bytes 131072

commit v4 on v3

--- a/solution.py
+++ b/solution.py
@@ -32,9 +32,10 @@
 UP = 384
 HID = 176
 W_AT = {2: [0], 6: [1], 8: [2]}
-W_KVY = {1: [3], 2: [4]}
+W_NEAR = {1: [3], 3: [4]}
 W_ATTN = {1: [5], 3: [6]}
 W_MORE = ([7, 8], [9, 10], [11, 12, 13, 14, 15, 16])
+NEAR = (-4, 6)
 TOK = 256
 
 
@@ -122,6 +123,8 @@
     owbuf,
     kvt,
     s_scr,
+    near_stats,
+    near_mixed,
     st_send,
     stats,
     o_send,
@@ -158,8 +161,8 @@
     vu,
     taps,
     loads,
-    kvs_z,
-    kvs_y,
+    unused,
+    kvs,
     kvr,
     qs,
     qr,
@@ -251,8 +254,8 @@
     def _(j):
         pl.semaphore_signal(barrier, inc=1, device_id=on_plane(j), device_id_type=MESH_IDS)
 
-    def kv_slot(yy, k):
-        start = pl.multiple_of((yy * NZ + k) * SHARE, SHARE)
+    def kv_slot(yy, d):
+        start = pl.multiple_of(((d + 8) * NY + yy) * SHARE, SHARE)
         return kvbuf.at[pl.ds(start, SHARE)]
 
     def w_slot(kind, core, k):
@@ -273,41 +276,38 @@
         ]
         turns[i] = jnp.concatenate(grid_rows, axis=0)
     rows = pl.ds(pl.multiple_of(tp * SHARE, SHARE), SHARE)
-    kv_slot(y, z)[:, :256] = rms_norm(
+    kv_slot(y, 0)[:, :256] = rms_norm(
         latent_v[...].astype(F32), in_one_row(kv_gain_v)
     ).astype(BF16)
     key_rows[...] = as_rows(rope_key_v[...])
-    kv_slot(y, z)[:, 256:] = turned(key_rows[rows], turns[0, rows], turns[1, rows]).astype(BF16)
+    kv_slot(y, 0)[:, 256:] = turned(key_rows[rows], turns[0, rows], turns[1, rows]).astype(BF16)
 
     pl.semaphore_wait(barrier, 5 + PLANE - 1)
-
-    pending = []
 
     def go(copy):
         copy.start()
-        pending.append(copy)
-
-    def kv_to(k, sem, dev):
-        slot = kv_slot(y, k)
-        go(push(slot, slot, kvs_z.at[sem], kvr.at[y * NZ + k], dev))
-
-    def kv_to_y(k, sem):
-        slot = kv_slot(y, k)
+
+    def kv_to(d, hop, dev):
+        seen = d - hop
+        go(push(kv_slot(y, d), kv_slot(y, seen), kvs.at[0], kvr.at[seen + 8], dev))
+
+    def kv_to_y(d):
+        slot = kv_slot(y, d)
         for j in range(1, NY):
             dev = (z, (y + j) % NY, x, c)
-            go(push(slot, slot, kvs_y.at[sem * 3 + j - 1], kvr.at[y * NZ + k], dev))
-
-    kv_to(z, 0, right2)
-    kv_to(z, 1, left2)
-    kv_to(z, 2, right)
-    kv_to(z, 3, left)
-    kv_to_y(z, 0)
+            go(push(slot, slot, kvs.at[0], kvr.at[16 if NEAR[0] <= d < NEAR[1] else 17], dev))
+
+    kv_to(0, 2, right2)
+    kv_to(0, -2, left2)
+    kv_to(0, 1, right)
+    kv_to(0, -1, left)
+    kv_to_y(0)
     ready("q_nope", "q_rope")
     qbuf[tp, :, :128] = q_nope_v[...]
     qbuf[tp, :, 128:] = turned(as_rows(q_rope_v[...]), turns[0], turns[1]).astype(BF16)
     for j in range(1, NT):
         t = (tp + j) % NT
-        go(push(qbuf.at[tp], qbuf.at[tp], qs.at[j - 1], qr.at[tp], tp_peer(t)))
+        go(push(qbuf.at[tp], qbuf.at[tp], qs.at[0], qr.at[0], tp_peer(t)))
 
     ready("up_value", "up_gate", "down")
     value, gate = up_value_v[...].astype(F32), up_gate_v[...].astype(F32)
@@ -321,41 +321,37 @@
     for j in range(1, NY):
         yy = (y + j) % NY
         dev = (z, yy, x, c)
-        go(push(w_loc.at[yy], w_part(0, y), wys.at[j - 1], wyr.at[y], dev))
-        go(push(d_loc.at[yy], w_part(1, y), wys.at[j + 2], wyr.at[NY + y], dev))
+        go(push(w_loc.at[yy], w_part(0, y), wys.at[0], wyr.at[0], dev))
+        go(push(d_loc.at[yy], w_part(1, y), wys.at[1], wyr.at[1], dev))
     w_part(0, y)[...] = w_loc[y]
     w_part(1, y)[...] = d_loc[y]
     dbuf[:, HID:] = jnp.zeros((NC, 256 - HID, D), BF16)
     ready("ow")
     go(push(owbuf.at[c], owbuf.at[c], ows.at[0], owr.at[0], partner))
 
-    def w_send(kind, k, step, to_right, to_left):
+    def w_send(kind, k, to_right, to_left):
         slot = w_slot(kind, c, k)
         if to_right:
-            go(push(slot, slot, wzs.at[kind, step], wzr.at[kind, k], right))
+            go(push(slot, slot, wzs.at[kind], wzr.at[kind, k], right))
         if to_left:
-            go(push(slot, slot, wzs.at[kind, 8 + step], wzr.at[kind, k], left))
-
-    def w_across(kind, k, sem):
+            go(push(slot, slot, wzs.at[kind], wzr.at[kind, k], left))
+
+    def w_across(kind, k):
         slot = w_slot(kind, c, k)
-        go(push(slot, slot, wps.at[kind, sem], wpr.at[kind, k], partner))
+        go(push(slot, slot, wps.at[kind], wpr.at[kind], partner))
 
     def w_wait(kind, k, dev):
         slot = w_slot(kind, c, k)
-        push(slot, slot, wzs.at[kind, 0], wzr.at[kind, k], dev).wait_recv()
+        push(slot, slot, wzs.at[kind], wzr.at[kind, k], dev).wait_recv()
 
     def w_start():
         for kind in range(2):
-            for j in range(1, NY):
-                yy = (y + j) % NY
-                part = w_part(kind, yy)
-                sem = wyr.at[kind * NY + yy]
-                push(part, part, wys.at[0], sem, (z, yy, x, c)).wait_recv()
+            landed((wbuf.at[c] if kind == 0 else d_stage).at[pl.ds(0, 96)], wyr.at[kind])
             if kind == 1:
                 columns = pl.ds(pl.multiple_of(z * ROWS, ROWS), ROWS)
                 dbuf[c, :HID, columns] = d_stage[...].astype(F32).T[:HID].astype(BF16)
-            w_send(kind, z, 0, True, True)
-            w_across(kind, z, 0)
+            w_send(kind, z, True, True)
+            w_across(kind, z)
 
     def w_go(steps):
         for event in steps:
@@ -365,22 +361,26 @@
             step, kind = (event + 1) // 2, (event + 1) % 2
             k = zz(-step)
             w_wait(kind, k, left)
-            w_send(kind, k, step, step < 8, False)
-            w_across(kind, k, 2 * step - 1)
+            w_send(kind, k, step < 8, False)
+            w_across(kind, k)
             if step < 8:
                 k = zz(step)
                 w_wait(kind, k, right)
-                w_send(kind, k, step, False, step < 7)
-                w_across(kind, k, 2 * step)
-
-    def kv_wait(yy, k):
-        slot = kv_slot(yy, k)
-        push(slot, slot, kvs_z.at[0], kvr.at[yy * NZ + k], right).wait_recv()
+                w_send(kind, k, False, step < 7)
+                w_across(kind, k)
+
+    def kv_wait(d):
+        slot = kv_slot(y, d)
+        push(slot, slot, kvs.at[0], kvr.at[d + 8], right).wait_recv()
+
+    def landed(ref, sem):
+        push(ref, ref, unused.at[0], sem, partner).wait_recv()
+
+    def left_here(ref, sem):
+        push(ref, ref, sem, unused.at[0], partner).wait_send()
 
     def fold_queries():
-        for j in range(1, NT):
-            t = (tp + j) % NT
-            push(qbuf.at[t], qbuf.at[t], qs.at[0], qr.at[t], tp_peer(t)).wait_recv()
+        landed(qbuf.at[pl.ds(0, NT - 1)], qr.at[0])
         ready("key_up")
         wide[...] = key_up_v[...].astype(F32)
         for h in range(NT):
@@ -404,40 +404,54 @@
             fold_queries()
         if d == 6:
             split_values()
-        k = zz(-d)
-        kv_wait(y, k)
+        kv_wait(-d)
         if d + 2 <= 8:
-            kv_to(k, 3 + d, right2)
+            kv_to(-d, 2, right2)
         if d < 8:
-            k2 = zz(d)
-            kv_wait(y, k2)
+            kv_wait(d)
             if d + 2 <= 7:
-                kv_to(k2, 9 + d, left2)
-        kv_to_y(k, 2 * d - 1)
+                kv_to(d, -2, left2)
+        kv_to_y(-d)
         if d < 8:
-            kv_to_y(k2, 2 * d)
+            kv_to_y(d)
         if d in W_AT:
             w_go(W_AT[d])
-    for j in range(1, NY):
-        yy = (y + j) % NY
-
-        @pl.loop(0, NZ)
-        def _(k):
-            kv_wait(yy, k)
-
-        if j in W_KVY:
-            w_go(W_KVY[j])
-
-    kvt[...] = kvbuf[:, :256].T
+    def weigh(hp, i, spans, top):
+        s_now = s_scr.at[i % 2]
+        for at in spans:
+            s_now[at] = dot_nt(kvbuf[at], qf[hp])
+            here = jnp.max(s_now[at], axis=0, keepdims=True)
+            top = here if top is None else jnp.maximum(top, here)
+        total, mixed = 0.0, 0.0
+        for at in spans:
+            weights = jnp.exp((s_now[at] - top) * scale)
+            total += jnp.sum(weights, axis=0, keepdims=True)
+            mixed += dot_nn(kvt[:, at], weights.astype(BF16))
+        return top, total, mixed
+
+    near, far = [slice(256, 896)], [slice(0, 256), slice(896, KEYS)]
+    landed(kvbuf.at[pl.ds(0, (NEAR[1] - NEAR[0]) * 3 * SHARE)], kvr.at[16])
+    for at in near:
+        kvt[:, at] = kvbuf[at, :256].T
+    for i in range(NX):
+        hp = (x + 1 + i) % NX
+        top, total, mixed = weigh(hp, i, near, None)
+        near_stats[i, 0:1] = top
+        near_stats[i, 1:2] = total
+        near_mixed[i] = mixed
+        if i in W_NEAR:
+            w_go(W_NEAR[i])
+    landed(kvbuf.at[pl.ds(0, (NZ - NEAR[1] + NEAR[0]) * 3 * SHARE)], kvr.at[17])
+    for at in far:
+        kvt[:, at] = kvbuf[at, :256].T
     lane = lax.broadcasted_iota(jnp.int32, (128, 256), 1)
     for i in range(NX):
         hp = (x + 1 + i) % NX
-        s_now = s_scr.at[i % 2]
-        s_now[...] = dot_nt(kvbuf[...], qf[hp])
-        top = jnp.max(s_now[...], axis=0, keepdims=True)
-        weights = jnp.exp((s_now[...] - top) * scale)
-        total = jnp.sum(weights, axis=0, keepdims=True)
-        mixed = dot_nn(kvt[...], weights.astype(BF16))
+        top_near = near_stats[i, 0:1]
+        top, total, mixed = weigh(hp, i, far, top_near)
+        factor = jnp.exp((top_near - top) * scale)
+        total += factor * near_stats[i, 1:2]
+        mixed += factor * near_mixed[i]
         mixed = dot_nn(vu[hp], mixed.astype(BF16))
         mixed = jnp.where((lane & 64) == 0, mixed[:128], mixed[128:]).astype(BF16)
         for core in range(NC):
@@ -449,23 +463,20 @@
         if i < NX - 1:
             for core in range(NC):
                 t = hp * NC + core
-                j = i * NC + core
-                go(push(st_send.at[t], stats.at[tp], sts.at[j], str_.at[tp], tp_peer(t)))
-                go(push(o_send.at[t], o_recv.at[tp], os_.at[j], or_.at[tp], tp_peer(t)))
+                go(push(st_send.at[t], stats.at[tp], sts.at[0], str_.at[0], tp_peer(t)))
+                go(push(o_send.at[t], o_recv.at[tp], os_.at[0], or_.at[0], tp_peer(t)))
         else:
             t = x * NC + 1 - c
-            go(push(st_send.at[t], stats.at[tp], sts.at[6], str_.at[tp], partner))
-            go(push(o_send.at[t], o_recv.at[tp], os_.at[6], or_.at[tp], partner))
+            go(push(st_send.at[t], stats.at[tp], sts.at[0], str_.at[0], partner))
+            go(push(o_send.at[t], o_recv.at[tp], os_.at[0], or_.at[0], partner))
             o_recv[tp] = o_send[tp]
             stats[tp] = st_send[tp]
         if i in W_ATTN:
             w_go(W_ATTN[i])
     w_go(W_MORE[0])
     push(owbuf.at[1 - c], owbuf.at[1 - c], ows.at[0], owr.at[0], partner).wait_recv()
-    for j in range(1, NT):
-        t = (tp + j) % NT
-        push(stats.at[t], stats.at[t], sts.at[0], str_.at[t], tp_peer(t)).wait_recv()
-        push(o_recv.at[t], o_recv.at[t], os_.at[0], or_.at[t], tp_peer(t)).wait_recv()
+    landed(stats.at[pl.ds(0, NT - 1)], str_.at[0])
+    landed(o_recv.at[pl.ds(0, NT - 1)], or_.at[0])
     top_all = stats[0, 0:1]
     for t in range(1, NT):
         top_all = jnp.maximum(top_all, stats[t, 0:1])
@@ -482,12 +493,10 @@
     for j in range(1, NX):
         xx = (x + j) % NX
         src = r_send.at[pl.ds(pl.multiple_of(xx * SHARE, SHARE), SHARE)]
-        go(push(src, r_recv.at[x], rss.at[j - 1], rsr.at[x], (z, y, xx, c)))
+        go(push(src, r_recv.at[x], rss.at[0], rsr.at[0], (z, y, xx, c)))
     r_recv[x] = r_send[pl.ds(pl.multiple_of(x * SHARE, SHARE), SHARE)]
     w_go(W_MORE[1])
-    for j in range(1, NX):
-        xx = (x + j) % NX
-        push(r_recv.at[xx], r_recv.at[xx], rss.at[0], rsr.at[xx], (z, y, xx, c)).wait_recv()
+    landed(r_recv.at[pl.ds(0, NX - 1)], rsr.at[0])
     ready("resid", "post", "pre", "ffn")
     summed = r_recv[0].astype(F32)
     for j in range(1, NX):
@@ -505,7 +514,7 @@
     def ag_copy(j):
         chip = (y * NX + x + j) % (NY * NX)
         dev = (z, chip // NX, chip % NX, half)
-        return push(in_send, in_slot(mine), ags.at[j], agr.at[mine], dev)
+        return push(in_send, in_slot(mine), ags.at[0], agr.at[0], dev)
 
     @pl.loop(1, NY * NX)
     def _(j):
@@ -532,18 +541,17 @@
         g = pltpu.roll(conv_v[1, :, lanes].astype(F32), back, 1)
         taps[core, 0:3] = jnp.concatenate(side_lanes(v[:, :HID], g[:, :HID]), axis=1)
 
-    @pl.loop(0, NZ)
-    def _(k):
-        slot = w_slot(0, 1 - c, k)
-        push(slot, slot, wps.at[0, 0], wpr.at[0, k], partner).wait_recv()
+    landed(wbuf.at[1 - c], wpr.at[0])
 
     own_slot = jnp.where(half == c, mine, -1)
 
-    @pl.loop(0, 16)
-    def _(s):
-        @pl.when(s != own_slot)
-        def _():
-            push(in_slot(s), in_slot(s), ags.at[0], agr.at[s], partner).wait_recv()
+    @pl.when(half == c)
+    def _():
+        landed(inbuf.at[pl.ds(0, 15 * SHARE)], agr.at[0])
+
+    @pl.when(half != c)
+    def _():
+        landed(inbuf, agr.at[0])
 
     for core in range(NC):
         up[core, 8 : 8 + TOK] = dot_nn(inbuf[...], wbuf[core])
@@ -570,10 +578,7 @@
         return (dot_nn(hidden[0], dbuf[0]) + dot_nn(hidden[1], dbuf[1])).astype(BF16)
 
     inner = [hidden_rows(core, SHARE, TOK - 2 * SHARE) for core in range(NC)]
-    @pl.loop(0, NZ)
-    def _(k):
-        slot = w_slot(1, 1 - c, k)
-        push(slot, slot, wps.at[1, 0], wpr.at[1, k], partner).wait_recv()
+    landed(dbuf.at[1 - c, pl.ds(0, HID)], wpr.at[1])
 
     p_send[SHARE : TOK - SHARE] = down_rows(inner)
 
@@ -584,7 +589,7 @@
 
     def rs_copy(s):
         dev = (z, 2 * c + s // NT, (s // NC) % NX, s % NC)
-        return push(p_slot(s), p_recv.at[chip], ps.at[s], pr.at[chip], dev)
+        return push(p_slot(s), p_recv.at[chip], ps.at[0], pr.at[0], dev)
 
     @pl.loop(0, 16)
     def _(j):
@@ -626,13 +631,13 @@
     def _():
         p_recv[chip] = p_slot(mine)[...]
 
-    own_chip = jnp.where(half == c, chip, -1)
-
-    @pl.loop(0, 16)
-    def _(k):
-        @pl.when(k != own_chip)
-        def _():
-            push(p_recv.at[k], p_recv.at[k], ps.at[0], pr.at[k], partner).wait_recv()
+    @pl.when(half == c)
+    def _():
+        landed(p_recv.at[pl.ds(0, 15)], pr.at[0])
+
+    @pl.when(half != c)
+    def _():
+        landed(p_recv, pr.at[0])
 
     projected = p_recv[0].astype(F32)
     for k in range(1, 16):
@@ -640,22 +645,31 @@
     projected = projected.astype(BF16).astype(F32)
     out[...] = (stream[...] + rms_norm(projected, in_one_row(gains.at[2]))).astype(BF16)
 
-    for copy in pending:
-        copy.wait_send()
-
-    @pl.loop(1, NY * NX)
-    def _(j):
-        ag_copy(j).wait_send()
+    left_here(kvbuf.at[pl.ds(0, 63 * SHARE)], kvs.at[0])
+    left_here(qbuf.at[pl.ds(0, NT - 1)], qs.at[0])
+    left_here(wbuf.at[0, pl.ds(0, 96)], wys.at[0])
+    left_here(d_stage.at[pl.ds(0, 96)], wys.at[1])
+    left_here(owbuf.at[0], ows.at[0])
+    left_here(wbuf.at[0, pl.ds(0, 15 * ROWS)], wzs.at[0])
+    left_here(dbuf.at[0, pl.ds(0, HID), pl.ds(0, 15 * ROWS)], wzs.at[1])
+    left_here(wbuf.at[0], wps.at[0])
+    left_here(dbuf.at[0, pl.ds(0, HID)], wps.at[1])
+    left_here(stats.at[pl.ds(0, NT - 1)], sts.at[0])
+    left_here(o_recv.at[pl.ds(0, NT - 1)], os_.at[0])
+    left_here(r_recv.at[pl.ds(0, NX - 1)], rss.at[0])
+    both = up.at[:, pl.ds(0, 8)]
+    left_here(both, hs.at[0])
+    left_here(both, hs.at[1])
+
+    @pl.when(half == c)
+    def _():
+        left_here(inbuf.at[pl.ds(0, 15 * SHARE)], ags.at[0])
+        left_here(p_send.at[pl.ds(0, 15 * SHARE)], ps.at[0])
 
     @pl.when(half != c)
     def _():
-        ag_copy(0).wait_send()
-
-    @pl.loop(0, 16)
-    def _(s):
-        @pl.when(s != own_slot)
-        def _():
-            rs_copy(s).wait_send()
+        left_here(inbuf, ags.at[0])
+        left_here(p_send, ps.at[0])
 
 
 def body(
@@ -696,6 +710,8 @@
             vmem((NC, 128, D), BF16),
             vmem((256, KEYS), BF16),
             vmem((2, KEYS, 256), F32),
+            vmem((NX, 8, 256), F32),
+            vmem((NX, 256, 256), F32),
             vmem((NT, 8, 128), F32),
             vmem((NT, 8, 128), F32),
             vmem((NT, 128, 128), BF16),
@@ -732,12 +748,9 @@
             vmem((4, 256, 256), BF16),
             vmem((NC, 8, UP), F32),
         ]
-        + [dma((n,)) for n in (19, 15, 48, 64, 7, 8, 6, 8)]
-        + [dma((2, 16))] * 4
-        + [
-            dma((n,))
-            for n in (1, 1, 7, 8, 7, 8, 3, 4, 16, 16, 2, 2, 16, 16)
-        ],
+        + [dma((n,)) for n in (19, 1, 1, 18, 1, 1, 2, 2, 2, 2)]
+        + [dma((2, NZ))]
+        + [dma((n,)) for n in (2, 1, 1, 1, 1, 1, 1, 1, 1, 1, 1, 2, 2, 1, 1)],
         compiler_params=pltpu.CompilerParams(
             collective_id=0, has_side_effects=True, vmem_limit_bytes=60 * 1024 * 1024
         ),

time: 85.1 us -> 82.4 us (0.968)
  Pallas kernels: 82.7 us -> 80.7 us
    pallas_call x1, Pallas kernels: 82.7 us -> 80.7 us  [body(): pl.pallas_call(functools.partial(layer_kernel, scale), out_shape=jax.Shap...]
where the time goes in v4:
time: 82.4 us; the launch traced here: 82.2 us
  Pallas kernels  80.7 us (98%)
  local copies, waits for them, and re-layouts  1.47 us (2%)
    pallas_call x1, Pallas kernels, body(): pl.pallas_call(functools.partial(layer_kernel, scale), out_shape=jax.Shap...  80.7 us

profile of v4, /device:TPU:1, one launch (start us, length us, event | category | flops | bytes accessed | tf_op | source)
XLA Modules:
  0.0 82.2 jit_solution(4098725038565200191)
XLA Ops:
  0.0 80.7 %layer.1 = bf16[16,2048]{1,0:T(8,128)(2,1)} custom-call(bf16[128,256]{1,0:T(8,128)(2,1)} %latent.1, bf16[64,128]{1,0:T(8,128)(2,1)} %bitcast.16, bf16[128,128]{1,0:T(8,128)(2,1)} %bitcast.15, bf16[64,128]{1,0:T(8,128)(2,1)} %bitcast.17, f32[64,8,128]{2,1,0:T(8,128)} %constant.4.clone.by_row, f32[2,64,128]{2,1,0:T(8,128)} %constant.5.clone.by_col, ...), custom_call_target="tpu_custom_call" | custom-call | tf_op jit(solution)/shard_map/layer/pallas_call | solution.py:699
  80.7 1.5 %copy.21 = bf16[16,2048]{1,0:T(8,128)(2,1)} copy(bf16[16,2048]{1,0:T(8,128)(2,1)} %layer.1) | data formatting | bytes 131072

commit v5 on v4

--- a/solution.py
+++ b/solution.py
@@ -31,10 +31,13 @@
 KW = 384
 UP = 384
 HID = 176
-W_AT = {2: [0], 6: [1], 8: [2]}
-W_NEAR = {1: [3], 3: [4]}
-W_ATTN = {1: [5], 3: [6]}
-W_MORE = ([7, 8], [9, 10], [11, 12, 13, 14, 15, 16])
+W_AT = {2: [0], 6: [1]}
+W_NEAR = {0: [2], 1: [3]}
+W_ATTN = {0: [4], 1: [5]}
+W_MORE = ([6, 7], [8, 9], [10, 11, 12, 13, 14, 15, 16])
+HOP = 3
+QG = 512
+NEAR_AT = 9
 NEAR = (-4, 6)
 TOK = 256
 
@@ -190,10 +193,10 @@
     z, y, x, c = (lax.axis_index(a) for a in AXES)
     tp = x * NC + c
     plane = y * NT + tp
-    half = y // 2
+    half = lax.div(y, 2)
 
     def zz(k):
-        return (z + k + NZ) % NZ
+        return lax.rem(z + k + NZ, NZ)
 
     def push(src, dst, ss, rs, dev):
         return pltpu.make_async_remote_copy(
@@ -203,15 +206,14 @@
 
     partner = (z, y, x, 1 - c)
     right, left = (zz(1), y, x, c), (zz(-1), y, x, c)
-    right2, left2 = (zz(2), y, x, c), (zz(-2), y, x, c)
     cross = ((z + 2 * c - 1 + NZ) % NZ, y, x, 1 - c)
 
     def on_plane(j):
-        p = (plane + j) % PLANE
-        return (z, p // NT, (p // NC) % NX, p % NC)
+        p = lax.rem(plane + j, PLANE)
+        return (z, lax.div(p, NT), lax.rem(lax.div(p, NC), NX), lax.rem(p, NC))
 
     def tp_peer(t):
-        return (z, y, t // NC, t % NC)
+        return (z, y, lax.div(t, NC), lax.rem(t, NC))
 
     def own(ref):
         return ref.at[pl.ds(pl.multiple_of(tp * SHARE, SHARE), SHARE)]
@@ -247,8 +249,10 @@
             local[name].wait()
 
     barrier = pltpu.get_barrier_semaphore()
-    for dev in (right, left, right2, left2, cross):
-        pl.semaphore_signal(barrier, inc=1, device_id=dev, device_id_type=MESH_IDS)
+    for hop in range(1, HOP + 1):
+        for dev in ((zz(hop), y, x, c), (zz(-hop), y, x, c)):
+            pl.semaphore_signal(barrier, inc=1, device_id=dev, device_id_type=MESH_IDS)
+    pl.semaphore_signal(barrier, inc=1, device_id=cross, device_id_type=MESH_IDS)
 
     @pl.loop(1, PLANE)
     def _(j):
@@ -282,7 +286,7 @@
     key_rows[...] = as_rows(rope_key_v[...])
     kv_slot(y, 0)[:, 256:] = turned(key_rows[rows], turns[0, rows], turns[1, rows]).astype(BF16)
 
-    pl.semaphore_wait(barrier, 5 + PLANE - 1)
+    pl.semaphore_wait(barrier, 2 * HOP + PLANE)
 
     def go(copy):
         copy.start()
@@ -294,19 +298,18 @@
     def kv_to_y(d):
         slot = kv_slot(y, d)
         for j in range(1, NY):
-            dev = (z, (y + j) % NY, x, c)
+            dev = (z, lax.rem(y + j, NY), x, c)
             go(push(slot, slot, kvs.at[0], kvr.at[16 if NEAR[0] <= d < NEAR[1] else 17], dev))
 
-    kv_to(0, 2, right2)
-    kv_to(0, -2, left2)
-    kv_to(0, 1, right)
-    kv_to(0, -1, left)
+    for hop in range(HOP, 0, -1):
+        kv_to(0, hop, (zz(hop), y, x, c))
+        kv_to(0, -hop, (zz(-hop), y, x, c))
     kv_to_y(0)
     ready("q_nope", "q_rope")
     qbuf[tp, :, :128] = q_nope_v[...]
     qbuf[tp, :, 128:] = turned(as_rows(q_rope_v[...]), turns[0], turns[1]).astype(BF16)
     for j in range(1, NT):
-        t = (tp + j) % NT
+        t = lax.rem(tp + j, NT)
         go(push(qbuf.at[tp], qbuf.at[tp], qs.at[0], qr.at[0], tp_peer(t)))
 
     ready("up_value", "up_gate", "down")
@@ -319,7 +322,7 @@
         parts = [across[:, at], jnp.zeros((32, 256 - HID), F32)]
         d_loc[yy] = jnp.concatenate(parts, axis=1).astype(BF16)
     for j in range(1, NY):
-        yy = (y + j) % NY
+        yy = lax.rem(y + j, NY)
         dev = (z, yy, x, c)
         go(push(w_loc.at[yy], w_part(0, y), wys.at[0], wyr.at[0], dev))
         go(push(d_loc.at[yy], w_part(1, y), wys.at[1], wyr.at[1], dev))
@@ -389,9 +392,10 @@
             folded = folded.reshape(NX, NC, SHARE, 256)
             rope = qbuf[h, :, 128:].reshape(NX, NC, SHARE, 128)
             for core in range(NC):
-                r = slice(core * 128 + h % 2 * 64, core * 128 + h % 2 * 64 + 64)
-                qf[h // 2, r, :256] = folded[:, core].reshape(64, 256)
-                qf[h // 2, r, 256:] = rope[:, core].reshape(64, 128)
+                first = (h // 2 * NC + core) * 128 + h % 2 * 64
+                r = slice(first, first + 64)
+                qf[r, :256] = folded[:, core].reshape(64, 256)
+                qf[r, 256:] = rope[:, core].reshape(64, 128)
 
     def split_values():
         ready("value_up")
@@ -399,80 +403,90 @@
         for h in range(NT):
             vu[h // 2, h % 2 * 128 : h % 2 * 128 + 128] = wide[pl.ds(h, 256, stride=NT)].T.astype(BF16)
 
+    def weigh(queries, spans, top):
+        for at in spans:
+            s_scr[at, queries] = dot_nt(kvbuf[at], qf[queries])
+            here = jnp.max(s_scr[at, queries], axis=0, keepdims=True)
+            top = here if top is None else jnp.maximum(top, here)
+        total, mixed = 0.0, 0.0
+        for at in spans:
+            weights = jnp.exp2((s_scr[at, queries] - top) * scale2)
+            total += jnp.sum(weights, axis=0, keepdims=True)
+            mixed += dot_nn(kvt[:, at], weights.astype(BF16))
+        return top, total, mixed
+
+    scale2 = scale * 1.4426950408889634
+    first, last = ((d + 8) * NY * SHARE for d in NEAR)
+    near, far = [slice(first, last)], [slice(0, first), slice(last, KEYS)]
+    groups = [slice(i * QG, (i + 1) * QG) for i in range(1024 // QG)]
+
+    def weigh_near():
+        landed(kvbuf.at[pl.ds(0, (NEAR[1] - NEAR[0]) * 3 * SHARE)], kvr.at[16])
+        for at in near:
+            kvt[:, at] = kvbuf[at, :256].T
+        for i, queries in enumerate(groups):
+            top, total, mixed = weigh(queries, near, None)
+            near_stats[0:1, queries] = top
+            near_stats[1:2, queries] = total
+            near_mixed[:, queries] = mixed
+            if i in W_NEAR:
+                w_go(W_NEAR[i])
+
     for d in range(1, 9):
         if d == 4:
             fold_queries()
         if d == 6:
             split_values()
+        if d == NEAR_AT:
+            weigh_near()
         kv_wait(-d)
-        if d + 2 <= 8:
-            kv_to(-d, 2, right2)
+        if d + HOP <= 8:
+            kv_to(-d, HOP, (zz(HOP), y, x, c))
         if d < 8:
             kv_wait(d)
-            if d + 2 <= 7:
-                kv_to(d, -2, left2)
+            if d + HOP <= 7:
+                kv_to(d, -HOP, (zz(-HOP), y, x, c))
         kv_to_y(-d)
         if d < 8:
             kv_to_y(d)
         if d in W_AT:
             w_go(W_AT[d])
-    def weigh(hp, i, spans, top):
-        s_now = s_scr.at[i % 2]
-        for at in spans:
-            s_now[at] = dot_nt(kvbuf[at], qf[hp])
-            here = jnp.max(s_now[at], axis=0, keepdims=True)
-            top = here if top is None else jnp.maximum(top, here)
-        total, mixed = 0.0, 0.0
-        for at in spans:
-            weights = jnp.exp((s_now[at] - top) * scale)
-            total += jnp.sum(weights, axis=0, keepdims=True)
-            mixed += dot_nn(kvt[:, at], weights.astype(BF16))
-        return top, total, mixed
-
-    near, far = [slice(256, 896)], [slice(0, 256), slice(896, KEYS)]
-    landed(kvbuf.at[pl.ds(0, (NEAR[1] - NEAR[0]) * 3 * SHARE)], kvr.at[16])
-    for at in near:
-        kvt[:, at] = kvbuf[at, :256].T
-    for i in range(NX):
-        hp = (x + 1 + i) % NX
-        top, total, mixed = weigh(hp, i, near, None)
-        near_stats[i, 0:1] = top
-        near_stats[i, 1:2] = total
-        near_mixed[i] = mixed
-        if i in W_NEAR:
-            w_go(W_NEAR[i])
+    if NEAR_AT == 9:
+        weigh_near()
     landed(kvbuf.at[pl.ds(0, (NZ - NEAR[1] + NEAR[0]) * 3 * SHARE)], kvr.at[17])
     for at in far:
         kvt[:, at] = kvbuf[at, :256].T
     lane = lax.broadcasted_iota(jnp.int32, (128, 256), 1)
-    for i in range(NX):
-        hp = (x + 1 + i) % NX
-        top_near = near_stats[i, 0:1]
-        top, total, mixed = weigh(hp, i, far, top_near)
-        factor = jnp.exp((top_near - top) * scale)
-        total += factor * near_stats[i, 1:2]
-        mixed += factor * near_mixed[i]
-        mixed = dot_nn(vu[hp], mixed.astype(BF16))
-        mixed = jnp.where((lane & 64) == 0, mixed[:128], mixed[128:]).astype(BF16)
-        for core in range(NC):
-            t = hp * NC + core
-            at = slice(core * 128, core * 128 + 128)
-            o_send[t] = mixed[:, at]
-            st_send[t, 0:1] = top[:, at]
-            st_send[t, 1:2] = total[:, at]
-        if i < NX - 1:
+    for i in range(2):
+        pair = (x // 2 + 1 + i) % 2
+        queries = pl.ds(pl.multiple_of(pair * QG, QG), QG)
+        top_near = near_stats[0:1, queries]
+        top, total, mixed = weigh(queries, far, top_near)
+        factor = jnp.exp2((top_near - top) * scale2)
+        total += factor * near_stats[1:2, queries]
+        mixed += factor * near_mixed[:, queries]
+        for k in range(2):
+            cut = slice(k * 256, k * 256 + 256)
+            part = dot_nn(vu[2 * pair + k], mixed[:, cut].astype(BF16))
+            part = jnp.where((lane & 64) == 0, part[:128], part[128:]).astype(BF16)
             for core in range(NC):
-                t = hp * NC + core
+                t = pair * 4 + k * NC + core
+                at = slice(core * 128, core * 128 + 128)
+                o_send[t] = part[:, at]
+                st_send[t, 0:1] = top[:, cut][:, at]
+                st_send[t, 1:2] = total[:, cut][:, at]
+        for k in range(4):
+            t = pair * 4 + (k + tp) % 4
+
+            @pl.when(t != tp)
+            def _():
                 go(push(st_send.at[t], stats.at[tp], sts.at[0], str_.at[0], tp_peer(t)))
                 go(push(o_send.at[t], o_recv.at[tp], os_.at[0], or_.at[0], tp_peer(t)))
-        else:
-            t = x * NC + 1 - c
-            go(push(st_send.at[t], stats.at[tp], sts.at[0], str_.at[0], partner))
-            go(push(o_send.at[t], o_recv.at[tp], os_.at[0], or_.at[0], partner))
-            o_recv[tp] = o_send[tp]
-            stats[tp] = st_send[tp]
+
         if i in W_ATTN:
             w_go(W_ATTN[i])
+    o_recv[tp] = o_send[tp]
+    stats[tp] = st_send[tp]
     w_go(W_MORE[0])
     push(owbuf.at[1 - c], owbuf.at[1 - c], ows.at[0], owr.at[0], partner).wait_recv()
     landed(stats.at[pl.ds(0, NT - 1)], str_.at[0])
@@ -483,7 +497,7 @@
     total_all = jnp.zeros_like(top_all)
     attended = jnp.zeros((128, 128), F32)
     for t in range(NT):
-        factor = jnp.exp((stats[t, 0:1] - top_all) * scale)
+        factor = jnp.exp2((stats[t, 0:1] - top_all) * scale2)
         total_all += factor * stats[t, 1:2]
         attended += factor * o_recv[t].astype(F32)
     attended = (attended / total_all).T.astype(BF16)
@@ -491,7 +505,7 @@
         dot_nn(attended[:64], owbuf[0]) + dot_nn(attended[64:], owbuf[1])
     ).astype(BF16)
     for j in range(1, NX):
-        xx = (x + j) % NX
+        xx = lax.rem(x + j, NX)
         src = r_send.at[pl.ds(pl.multiple_of(xx * SHARE, SHARE), SHARE)]
         go(push(src, r_recv.at[x], rss.at[0], rsr.at[0], (z, y, xx, c)))
     r_recv[x] = r_send[pl.ds(pl.multiple_of(x * SHARE, SHARE), SHARE)]
@@ -512,8 +526,8 @@
     mine = (y % 2) * NT + tp
 
     def ag_copy(j):
-        chip = (y * NX + x + j) % (NY * NX)
-        dev = (z, chip // NX, chip % NX, half)
+        chip = lax.rem(y * NX + x + j, NY * NX)
+        dev = (z, lax.div(chip, NX), lax.rem(chip, NX), half)
         return push(in_send, in_slot(mine), ags.at[0], agr.at[0], dev)
 
     @pl.loop(1, NY * NX)
@@ -588,12 +602,12 @@
         return p_send.at[pl.ds(pl.multiple_of(s * SHARE, SHARE), SHARE)]
 
     def rs_copy(s):
-        dev = (z, 2 * c + s // NT, (s // NC) % NX, s % NC)
+        dev = (z, 2 * c + lax.div(s, NT), lax.rem(lax.div(s, NC), NX), lax.rem(s, NC))
         return push(p_slot(s), p_recv.at[chip], ps.at[0], pr.at[0], dev)
 
     @pl.loop(0, 16)
     def _(j):
-        s = (mine + j) % 16
+        s = lax.rem(mine + j, 16)
 
         @pl.when((s != own_slot) & (s > 0) & (s < 15))
         def _():
@@ -709,9 +723,9 @@
             vmem((ROWS, 256), BF16),
             vmem((NC, 128, D), BF16),
             vmem((256, KEYS), BF16),
-            vmem((2, KEYS, 256), F32),
-            vmem((NX, 8, 256), F32),
-            vmem((NX, 256, 256), F32),
+            vmem((KEYS, 1024), F32),
+            vmem((8, 1024), F32),
+            vmem((256, 1024), F32),
             vmem((NT, 8, 128), F32),
             vmem((NT, 8, 128), F32),
             vmem((NT, 128, 128), BF16),
@@ -744,7 +758,7 @@
             vmem((NY, 32, UP), BF16),
             vmem((NY, 32, 256), BF16),
             vmem((256 * NT, 128), F32),
-            vmem((4, 256, KW), BF16),
+            vmem((NX * 256, KW), BF16),
             vmem((4, 256, 256), BF16),
             vmem((NC, 8, UP), F32),
         ]

time: 82.4 us -> 79 us (0.959)
  the two profiles are of different devices: /device:TPU:1 before, /device:TPU:32 now
where the time goes in v5:
time: 79 us; the launch traced here: 78.9 us
  Pallas kernels  77.4 us (98%)
  local copies, waits for them, and re-layouts  1.47 us (2%)
    pallas_call x1, Pallas kernels, body(): pl.pallas_call(functools.partial(layer_kernel, scale), out_shape=jax.Shap...  77.4 us

profile of v5, /device:TPU:32, one launch (start us, length us, event | category | flops | bytes accessed | tf_op | source)
XLA Modules:
  0.0 78.9 jit_solution(10192377917460337486)
XLA Ops:
  0.0 77.4 %layer.1 = bf16[16,2048]{1,0:T(8,128)(2,1)} custom-call(bf16[128,256]{1,0:T(8,128)(2,1)} %latent.1, bf16[64,128]{1,0:T(8,128)(2,1)} %bitcast.16, bf16[128,128]{1,0:T(8,128)(2,1)} %bitcast.15, bf16[64,128]{1,0:T(8,128)(2,1)} %bitcast.17, f32[64,8,128]{2,1,0:T(8,128)} %constant.4.clone.by_row, f32[2,64,128]{2,1,0:T(8,128)} %constant.5.clone.by_col, ...), custom_call_target="tpu_custom_call" | custom-call | tf_op jit(solution)/shard_map/layer/pallas_call | solution.py:713
  77.4 1.5 %copy.21 = bf16[16,2048]{1,0:T(8,128)(2,1)} copy(bf16[16,2048]{1,0:T(8,128)(2,1)} %layer.1) | data formatting | bytes 131072

commit v6 on v5

--- a/solution.py
+++ b/solution.py
@@ -138,7 +138,11 @@
     inbuf,
     up,
     p_send,
-    p_recv,
+    a_recv,
+    b_recv,
+    a_send,
+    b_send,
+    fin,
     stream,
     latent_v,
     rope_key_v,
@@ -228,10 +232,40 @@
     load("rope_key", rope_key, rope_key_v)
     load("by_row", by_row.at[z * NY + y], by_row_v)
     load("by_col", by_col, by_col_v)
-    load("kv_gain", kv_gain, kv_gain_v)
     load("post", post_gain, gains.at[0])
     load("pre", pre_gain, gains.at[1])
     load("ffn", ffn_gain, gains.at[2])
+    load("kv_gain", kv_gain, kv_gain_v)
+
+    def ready(*names):
+        for name in names:
+            local[name].wait()
+
+    barrier = pltpu.get_barrier_semaphore()
+    for hop in range(1, HOP + 1):
+        for dev in ((zz(hop), y, x, c), (zz(-hop), y, x, c)):
+            pl.semaphore_signal(barrier, inc=1, device_id=dev, device_id_type=MESH_IDS)
+    pl.semaphore_signal(barrier, inc=1, device_id=cross, device_id_type=MESH_IDS)
+
+    @pl.loop(1, PLANE)
+    def _(j):
+        pl.semaphore_signal(barrier, inc=1, device_id=on_plane(j), device_id_type=MESH_IDS)
+
+    def kv_slot(yy, d):
+        start = pl.multiple_of(((d + 8) * NY + yy) * SHARE, SHARE)
+        return kvbuf.at[pl.ds(start, SHARE)]
+
+    def w_slot(kind, core, k):
+        at = pl.ds(pl.multiple_of(k * ROWS, ROWS), ROWS)
+        if kind == 0:
+            return wbuf.at[core, at]
+        return dbuf.at[core, pl.ds(0, HID), at]
+
+    def w_part(kind, yy):
+        if kind == 0:
+            return wbuf.at[c, pl.ds(pl.multiple_of(z * ROWS + yy * 32, 32), 32)]
+        return d_stage.at[pl.ds(pl.multiple_of(yy * 32, 32), 32)]
+
     load("q_nope", q_nope, q_nope_v)
     load("q_rope", q_rope, q_rope_v)
     load("up_value", up_value, up_value_v)
@@ -243,35 +277,6 @@
     load("resid", own(resid), resid_v)
     load("conv_value", conv_value, conv_v.at[0])
     load("conv_gate", conv_gate, conv_v.at[1])
-
-    def ready(*names):
-        for name in names:
-            local[name].wait()
-
-    barrier = pltpu.get_barrier_semaphore()
-    for hop in range(1, HOP + 1):
-        for dev in ((zz(hop), y, x, c), (zz(-hop), y, x, c)):
-            pl.semaphore_signal(barrier, inc=1, device_id=dev, device_id_type=MESH_IDS)
-    pl.semaphore_signal(barrier, inc=1, device_id=cross, device_id_type=MESH_IDS)
-
-    @pl.loop(1, PLANE)
-    def _(j):
-        pl.semaphore_signal(barrier, inc=1, device_id=on_plane(j), device_id_type=MESH_IDS)
-
-    def kv_slot(yy, d):
-        start = pl.multiple_of(((d + 8) * NY + yy) * SHARE, SHARE)
-        return kvbuf.at[pl.ds(start, SHARE)]
-
-    def w_slot(kind, core, k):
-        at = pl.ds(pl.multiple_of(k * ROWS, ROWS), ROWS)
-        if kind == 0:
-            return wbuf.at[core, at]
-        return dbuf.at[core, pl.ds(0, HID), at]
-
-    def w_part(kind, yy):
-        if kind == 0:
-            return wbuf.at[c, pl.ds(pl.multiple_of(z * ROWS + yy * 32, 32), 32)]
-        return d_stage.at[pl.ds(pl.multiple_of(yy * 32, 32), 32)]
 
     ready("latent", "rope_key", "by_row", "by_col", "kv_gain")
     for i in range(2):
@@ -557,7 +562,6 @@
 
     landed(wbuf.at[1 - c], wpr.at[0])
 
-    own_slot = jnp.where(half == c, mine, -1)
 
     @pl.when(half == c)
     def _():
@@ -596,22 +600,36 @@
 
     p_send[SHARE : TOK - SHARE] = down_rows(inner)
 
-    chip = y * NX + x
-
-    def p_slot(s):
-        return p_send.at[pl.ds(pl.multiple_of(s * SHARE, SHARE), SHARE)]
-
-    def rs_copy(s):
-        dev = (z, 2 * c + lax.div(s, NT), lax.rem(lax.div(s, NC), NX), lax.rem(s, NC))
-        return push(p_slot(s), p_recv.at[chip], ps.at[0], pr.at[0], dev)
+    left_cols, right_cols = pl.ds(0, D // 2), pl.ds(D // 2, D // 2)
+    yl = lax.rem(y, 2)
+
+    def along_x(s):
+        to = lax.rem(lax.div(s, NC), NX)
+        src = p_send.at[pl.ds(pl.multiple_of(s * SHARE, SHARE), SHARE), left_cols]
+        at = pl.multiple_of((lax.div(s, NT) * NC + lax.rem(s, NC)) * SHARE, SHARE)
+        dst = a_recv.at[x, pl.ds(at, SHARE)]
+        return to, push(src, dst, ps.at[0], pr.at[0], (z, y, to, c))
+
+    def along_y(k, first, count):
+        at = pl.ds(pl.multiple_of(k * ROWS + first, SHARE), count)
+        dst = b_recv.at[y, pl.ds(first, count)]
+        dev = (z, 2 * c + k, x, c)
+        return push(p_send.at[at, right_cols], dst, ps.at[1], pr.at[1], dev)
+
+    for k, first in ((0, SHARE), (1, 0)):
+
+        @pl.when(2 * c + k != y)
+        def _():
+            along_y(k, first, ROWS - SHARE).start()
 
     @pl.loop(0, 16)
     def _(j):
-        s = lax.rem(mine + j, 16)
-
-        @pl.when((s != own_slot) & (s > 0) & (s < 15))
+        s = lax.rem(mine + 2 + j, 16)
+        to, copy = along_x(s)
+
+        @pl.when((to != x) & (s > 0) & (s < 15))
         def _():
-            rs_copy(s).start()
+            copy.start()
 
     low, high = up.at[:, pl.ds(0, 8)], up.at[:, pl.ds(TOK + 8, 8)]
     push(low, low, hs.at[0], hr.at[0], low_dev).wait_recv()
@@ -634,29 +652,74 @@
     edges = down_rows(outer)
     p_send[:SHARE] = edges[:SHARE]
     p_send[TOK - SHARE :] = edges[SHARE:]
-    for s in (0, 15):
-
-        @pl.when(s != own_slot)
+    for k, first, s in ((0, 0, 0), (1, ROWS - SHARE, 15)):
+
+        @pl.when(2 * c + k != y)
         def _():
-            rs_copy(s).start()
-
+            along_y(k, first, SHARE).start()
+
+        to, copy = along_x(jnp.int32(s))
+
+        @pl.when(to != x)
+        def _():
+            copy.start()
+
+    def own_part(k, first, count, cols):
+        at = pl.multiple_of(k * ROWS + first, SHARE)
+        return p_send[pl.ds(at, count), cols].astype(F32)
+
+    landed(a_recv.at[pl.ds(0, NX - 1)], pr.at[0])
+    total = jnp.concatenate([own_part(k, x * 32, 32, left_cols) for k in range(2)], axis=0)
+    for j in range(1, NX):
+        total += a_recv[lax.rem(x + j, NX)].astype(F32)
+    a_send[...] = total.astype(BF16)
+
+    def a_owner(k, core):
+        at = (k * NC + core) * SHARE
+        dev = (z, 2 * c + k, x, core)
+        return push(a_send.at[pl.ds(at, SHARE)], fin.at[0, y], ps.at[2], pr.at[2], dev)
+
+    for k in range(2):
+        for core in range(NC):
+
+            @pl.when((2 * c + k != y) | (c != core))
+            def _():
+                a_owner(k, core).start()
+
+    def b_owner(j):
+        t = lax.rem(tp + j, NT)
+        at = pl.multiple_of(t * SHARE, SHARE)
+        return push(b_send.at[pl.ds(at, SHARE)], fin.at[1, x], ps.at[3], pr.at[3], tp_peer(t))
 
     @pl.when(half == c)
     def _():
-        p_recv[chip] = p_slot(mine)[...]
-
-    @pl.when(half == c)
-    def _():
-        landed(p_recv.at[pl.ds(0, 15)], pr.at[0])
-
-    @pl.when(half != c)
-    def _():
-        landed(p_recv, pr.at[0])
-
-    projected = p_recv[0].astype(F32)
-    for k in range(1, 16):
-        projected += p_recv[k].astype(F32)
-    projected = projected.astype(BF16).astype(F32)
+        landed(b_recv.at[pl.ds(0, NY - 1)], pr.at[1])
+        total = own_part(yl, 0, ROWS, right_cols)
+        for j in range(1, NY):
+            total += b_recv[lax.rem(y + j, NY)].astype(F32)
+        b_send[...] = total.astype(BF16)
+        for j in range(1, NT):
+            b_owner(j).start()
+        fin[1, x] = b_send[pl.ds(pl.multiple_of(tp * SHARE, SHARE), SHARE)]
+        fin[0, y] = a_send[pl.ds(pl.multiple_of((yl * NC + c) * SHARE, SHARE), SHARE)]
+
+    for kind in range(2):
+
+        @pl.when(half == c)
+        def _():
+            landed(fin.at[kind, pl.ds(0, 3)], pr.at[2 + kind])
+
+        @pl.when(half != c)
+        def _():
+            landed(fin.at[kind], pr.at[2 + kind])
+
+    sums = []
+    for kind in range(2):
+        part = fin[kind, 0].astype(F32)
+        for k in range(1, 4):
+            part += fin[kind, k].astype(F32)
+        sums.append(part)
+    projected = jnp.concatenate(sums, axis=1).astype(BF16).astype(F32)
     out[...] = (stream[...] + rms_norm(projected, in_one_row(gains.at[2]))).astype(BF16)
 
     left_here(kvbuf.at[pl.ds(0, 63 * SHARE)], kvs.at[0])
@@ -671,6 +734,7 @@
     left_here(stats.at[pl.ds(0, NT - 1)], sts.at[0])
     left_here(o_recv.at[pl.ds(0, NT - 1)], os_.at[0])
     left_here(r_recv.at[pl.ds(0, NX - 1)], rss.at[0])
+    left_here(a_recv.at[pl.ds(0, NX - 1)], ps.at[0])
     both = up.at[:, pl.ds(0, 8)]
     left_here(both, hs.at[0])
     left_here(both, hs.at[1])
@@ -678,12 +742,15 @@
     @pl.when(half == c)
     def _():
         left_here(inbuf.at[pl.ds(0, 15 * SHARE)], ags.at[0])
-        left_here(p_send.at[pl.ds(0, 15 * SHARE)], ps.at[0])
+        left_here(b_recv.at[0], ps.at[1])
+        left_here(fin.at[0, pl.ds(0, 3)], ps.at[2])
+        left_here(b_send.at[pl.ds(0, 7 * SHARE)], ps.at[3])
 
     @pl.when(half != c)
     def _():
         left_here(inbuf, ags.at[0])
-        left_here(p_send, ps.at[0])
+        left_here(b_recv.at[pl.ds(0, 2)], ps.at[1])
+        left_here(fin.at[0], ps.at[2])
 
 
 def body(
@@ -736,7 +803,11 @@
             vmem((TOK, D), BF16),
             vmem((NC, TOK + 16, UP), F32),
             vmem((TOK, D), BF16),
-            vmem((NY * NX, SHARE, D), BF16),
+            vmem((NX, 64, D // 2), BF16),
+            vmem((NY, ROWS, D // 2), BF16),
+            vmem((64, D // 2), BF16),
+            vmem((ROWS, D // 2), BF16),
+            vmem((2, 4, SHARE, D // 2), BF16),
             vmem((SHARE, D), F32),
             vmem((SHARE, 256), BF16),
             vmem((64, ROWS), BF16),
@@ -764,7 +835,7 @@
         ]
         + [dma((n,)) for n in (19, 1, 1, 18, 1, 1, 2, 2, 2, 2)]
         + [dma((2, NZ))]
-        + [dma((n,)) for n in (2, 1, 1, 1, 1, 1, 1, 1, 1, 1, 1, 2, 2, 1, 1)],
+        + [dma((n,)) for n in (2, 1, 1, 1, 1, 1, 1, 1, 1, 1, 1, 2, 2, 4, 4)],
         compiler_params=pltpu.CompilerParams(
             collective_id=0, has_side_effects=True, vmem_limit_bytes=60 * 1024 * 1024
         ),

time: 79 us -> 78.1 us (0.989)
  the two profiles are of different devices: /device:TPU:32 before, /device:TPU:1 now
where the time goes in v6:
time: 78.1 us; the launch traced here: 78 us
  Pallas kernels  76.5 us (98%)
  local copies, waits for them, and re-layouts  1.47 us (2%)
    pallas_call x1, Pallas kernels, body(): pl.pallas_call(functools.partial(layer_kernel, scale), out_shape=jax.Shap...  76.5 us

profile of v6, /device:TPU:1, one launch (start us, length us, event | category | flops | bytes accessed | tf_op | source)
XLA Modules:
  0.0 78.0 jit_solution(6896949910442973366)
XLA Ops:
  0.0 76.5 %layer.1 = bf16[16,2048]{1,0:T(8,128)(2,1)} custom-call(bf16[128,256]{1,0:T(8,128)(2,1)} %latent.1, bf16[64,128]{1,0:T(8,128)(2,1)} %bitcast.16, bf16[128,128]{1,0:T(8,128)(2,1)} %bitcast.15, bf16[64,128]{1,0:T(8,128)(2,1)} %bitcast.17, f32[64,8,128]{2,1,0:T(8,128)} %constant.4.clone.by_row, f32[2,64,128]{2,1,0:T(8,128)} %constant.5.clone.by_col, ...), custom_call_target="tpu_custom_call" | custom-call | tf_op jit(solution)/shard_map/layer/pallas_call | solution.py:780
  76.5 1.5 %copy.21 = bf16[16,2048]{1,0:T(8,128)(2,1)} copy(bf16[16,2048]{1,0:T(8,128)(2,1)} %layer.1) | data formatting | bytes 131072

commit v7 on v6

--- a/solution.py
+++ b/solution.py
@@ -31,7 +31,7 @@
 KW = 384
 UP = 384
 HID = 176
-W_AT = {2: [0], 6: [1]}
+W_AT = {2: [0], 5: [1]}
 W_NEAR = {0: [2], 1: [3]}
 W_ATTN = {0: [4], 1: [5]}
 W_MORE = ([6, 7], [8, 9], [10, 11, 12, 13, 14, 15, 16])
@@ -247,9 +247,12 @@
             pl.semaphore_signal(barrier, inc=1, device_id=dev, device_id_type=MESH_IDS)
     pl.semaphore_signal(barrier, inc=1, device_id=cross, device_id_type=MESH_IDS)
 
-    @pl.loop(1, PLANE)
-    def _(j):
-        pl.semaphore_signal(barrier, inc=1, device_id=on_plane(j), device_id_type=MESH_IDS)
+    for j in range(1, NY):
+        dev = (z, lax.rem(y + j, NY), x, c)
+        pl.semaphore_signal(barrier, inc=1, device_id=dev, device_id_type=MESH_IDS)
+    for j in range(1, NT):
+        dev = tp_peer(lax.rem(tp + j, NT))
+        pl.semaphore_signal(barrier, inc=1, device_id=dev, device_id_type=MESH_IDS)
 
     def kv_slot(yy, d):
         start = pl.multiple_of(((d + 8) * NY + yy) * SHARE, SHARE)
@@ -291,7 +294,7 @@
     key_rows[...] = as_rows(rope_key_v[...])
     kv_slot(y, 0)[:, 256:] = turned(key_rows[rows], turns[0, rows], turns[1, rows]).astype(BF16)
 
-    pl.semaphore_wait(barrier, 2 * HOP + PLANE)
+    pl.semaphore_wait(barrier, 2 * HOP + NY + NT - 1)
 
     def go(copy):
         copy.start()

time: 78.1 us -> 76.7 us (0.982)
  Pallas kernels: 76.5 us -> 75 us
    pallas_call x1, Pallas kernels: 76.5 us -> 75 us  [body(): pl.pallas_call(functools.partial(layer_kernel, scale), out_shape=jax.Shap...]
where the time goes in v7:
time: 76.7 us; the launch traced here: 76.5 us
  Pallas kernels  75 us (98%)
  local copies, waits for them, and re-layouts  1.47 us (2%)
    pallas_call x1, Pallas kernels, body(): pl.pallas_call(functools.partial(layer_kernel, scale), out_shape=jax.Shap...  75 us

profile of v7, /device:TPU:1, one launch (start us, length us, event | category | flops | bytes accessed | tf_op | source)
XLA Modules:
  0.0 76.5 jit_solution(9169356454973131809)
XLA Ops:
  0.0 75.0 %layer.1 = bf16[16,2048]{1,0:T(8,128)(2,1)} custom-call(bf16[128,256]{1,0:T(8,128)(2,1)} %latent.1, bf16[64,128]{1,0:T(8,128)(2,1)} %bitcast.16, bf16[128,128]{1,0:T(8,128)(2,1)} %bitcast.15, bf16[64,128]{1,0:T(8,128)(2,1)} %bitcast.17, f32[64,8,128]{2,1,0:T(8,128)} %constant.4.clone.by_row, f32[2,64,128]{2,1,0:T(8,128)} %constant.5.clone.by_col, ...), custom_call_target="tpu_custom_call" | custom-call | tf_op jit(solution)/shard_map/layer/pallas_call | solution.py:783
  75.1 1.5 %copy.21 = bf16[16,2048]{1,0:T(8,128)(2,1)} copy(bf16[16,2048]{1,0:T(8,128)(2,1)} %layer.1) | data formatting | bytes 131072

commit v8 on v7

--- a/solution.py
+++ b/solution.py
@@ -595,13 +595,14 @@
         far = jnp.where(lane < 64, far, 0.0)
         return jnp.concatenate([near.astype(BF16), far.astype(BF16)], axis=1)
 
-    def down_rows(hidden):
-        return (dot_nn(hidden[0], dbuf[0]) + dot_nn(hidden[1], dbuf[1])).astype(BF16)
+    def down_rows(hidden, cols):
+        total = dot_nn(hidden[0], dbuf[0, :, cols]) + dot_nn(hidden[1], dbuf[1, :, cols])
+        return total.astype(BF16)
 
     inner = [hidden_rows(core, SHARE, TOK - 2 * SHARE) for core in range(NC)]
     landed(dbuf.at[1 - c, pl.ds(0, HID)], wpr.at[1])
 
-    p_send[SHARE : TOK - SHARE] = down_rows(inner)
+    p_send[SHARE : TOK - SHARE, D // 2 :] = down_rows(inner, slice(D // 2, D))
 
     left_cols, right_cols = pl.ds(0, D // 2), pl.ds(D // 2, D // 2)
     yl = lax.rem(y, 2)
@@ -625,6 +626,8 @@
         def _():
             along_y(k, first, ROWS - SHARE).start()
 
+    p_send[SHARE : TOK - SHARE, : D // 2] = down_rows(inner, slice(0, D // 2))
+
     @pl.loop(0, 16)
     def _(j):
         s = lax.rem(mine + 2 + j, 16)
@@ -652,7 +655,7 @@
         )
         for core in range(NC)
     ]
-    edges = down_rows(outer)
+    edges = down_rows(outer, slice(0, D))
     p_send[:SHARE] = edges[:SHARE]
     p_send[TOK - SHARE :] = edges[SHARE:]
     for k, first, s in ((0, 0, 0), (1, ROWS - SHARE, 15)):

time: 76.7 us -> 76.5 us (level)
  no operation moved by 1% of the time
where the time goes in v8:
time: 76.5 us; the launch traced here: 76.3 us
  Pallas kernels  74.8 us (98%)
  local copies, waits for them, and re-layouts  1.47 us (2%)
    pallas_call x1, Pallas kernels, body(): pl.pallas_call(functools.partial(layer_kernel, scale), out_shape=jax.Shap...  74.8 us

profile of v8, /device:TPU:1, one launch (start us, length us, event | category | flops | bytes accessed | tf_op | source)
XLA Modules:
  0.0 76.3 jit_solution(14005271886864509036)
XLA Ops:
  0.0 74.8 %layer.1 = bf16[16,2048]{1,0:T(8,128)(2,1)} custom-call(bf16[128,256]{1,0:T(8,128)(2,1)} %latent.1, bf16[64,128]{1,0:T(8,128)(2,1)} %bitcast.16, bf16[128,128]{1,0:T(8,128)(2,1)} %bitcast.15, bf16[64,128]{1,0:T(8,128)(2,1)} %bitcast.17, f32[64,8,128]{2,1,0:T(8,128)} %constant.4.clone.by_row, f32[2,64,128]{2,1,0:T(8,128)} %constant.5.clone.by_col, ...), custom_call_target="tpu_custom_call" | custom-call | tf_op jit(solution)/shard_map/layer/pallas_call | solution.py:786
  74.8 1.5 %copy.21 = bf16[16,2048]{1,0:T(8,128)(2,1)} copy(bf16[16,2048]{1,0:T(8,128)(2,1)} %layer.1) | data formatting | bytes 131072
